TPU v7x, 32 devices: a whole 2x2x4 slice. The times are simulated.
32 devices in a mesh: sp: 8 (over z, x), dp: 4 (over y, core).
Axes of the slice: x: 2, y: 2, z: 4, core: 2. Of those that a mesh axis runs over, the one named last changes fastest.
Arguments:
- hidden_in: bfloat16 [4, 1024, 2048], P('dp', 'sp'), may hold values from -6 to 6
- mix_cotangent: bfloat16 [4, 1024, 4096], P('dp', 'sp'), may hold values from -0.119628906 to 0.119628906
- query_weight: bfloat16 [2048, 4096], P('dp', 'sp'), may hold values from -0.125 to 0.125
- key_weight: bfloat16 [2048, 4096], P('dp', 'sp'), may hold values from -0.125 to 0.125
- value_weight: bfloat16 [2048, 4096], P('dp', 'sp'), may hold values from -0.125 to 0.125
- decay_log: float32 [16], P('sp'), may hold values from -0.034 to -0.00029296875, as said below
Outputs:
- grad_hidden: bfloat16 [4, 1024, 2048], P('dp', 'sp')
- grad_query: float32 [2048, 4096], P('dp', 'sp')
- grad_key: float32 [2048, 4096], P('dp', 'sp')
- grad_value: float32 [2048, 4096], P('dp', 'sp')
Inputs may be any that keep to these rules, and one draw needn't show every extreme that they name: Each head's decay_log is negative.
All inputs are finite; a program needn't handle non-finite values.
Results may differ from a plain program's by a relative error of at most 0.015.
Values may be sent and summed in bfloat16 or wider, within the bound.
A program may use at most 64 MiB of HBM per device.

v0:
```python
import functools

import jax
import jax.numpy as jnp
from jax import lax
from jax.experimental import pallas as pl
from jax.experimental.pallas import tpu as pltpu
from jax.sharding import PartitionSpec as P

BLOCK = 128
SUBS = 2
F32 = jnp.float32
BF16 = jnp.bfloat16
MESH = pl.DeviceIdType.MESH
NT = (((1,), (1,)), ((), ()))
TN = (((0,), (0,)), ((), ()))
VMEM_LIMIT = 52 * 1024 * 1024


def dot(a, b, dims=(((1,), (0,)), ((), ()))):
    return lax.dot_general(a, b, dims, preferred_element_type=F32)


def remote(src, dst, send, recv, where):
    return pltpu.make_async_remote_copy(
        src_ref=src, dst_ref=dst, send_sem=send, recv_sem=recv, device_id=where, device_id_type=MESH
    )


def greet(targets):
    barrier = pltpu.get_barrier_semaphore()
    for where in targets:
        pl.semaphore_signal(barrier, inc=1, device_id=where, device_id_type=MESH)
    pl.semaphore_wait(barrier, len(targets))


def gather_phase(
    n, m, project, h_in, c_in, wq, wk, wv, h_all, c_all, w_all,
    h_recv, h_line, h_side, c_send, c_recv, w_far, w_near, w_recv,
):
    s = lax.axis_index("sp")
    d = lax.axis_index("dp")
    z, x = s // 2, s % 2
    y, core = d // 2, d % 2
    nz, ny = n // 2, m // 2
    rows = h_in.shape[0]
    sub_rows = rows // SUBS
    depth, columns = wq.shape
    side = s + 1 - 2 * x
    mate = d + 1 - 2 * core

    def far(o):
        return ((y + o) % ny) * 2 + core

    greet(
        [{"sp": (s + k) % n} for k in range(1, n)]
        + [{"dp": mate}]
        + [{"dp": far(o)} for o in range(1, ny)]
    )

    def h_copy(src_z, src_x, sub, dest, send, own=False):
        block = src_z * 2 + src_x
        place = pl.ds(pl.multiple_of(block * rows + sub * sub_rows, sub_rows), sub_rows)
        src = h_in.at[pl.ds(sub * sub_rows, sub_rows)] if own else h_all.at[place]
        return remote(src, h_all.at[place], send, h_recv.at[block, sub], {"sp": dest})

    def w_copy(src_d, j, dest, send, own=False):
        place = w_all.at[
            pl.ds(pl.multiple_of(src_d * depth, depth), depth), pl.ds(j * columns, columns)
        ]
        return remote((wq, wk, wv)[j] if own else place, place, send, w_recv.at[src_d, j], {"dp": dest})

    def c_copy(k):
        to = (s + k) % n
        return remote(
            c_in.at[:, pl.ds(pl.multiple_of(to * columns, columns), columns)],
            c_all.at[pl.ds(pl.multiple_of(s * rows, rows), rows)],
            c_send.at[k - 1],
            c_recv.at[k - 1],
            {"sp": to},
        )

    def line(k, sub, up, own):
        source = (z - k) if up else (z + k)
        dest = (s + 2) if up else (s - 2)
        return h_copy(source, x, sub, dest, h_line.at[k, sub, int(up)], own)

    def goes(k, up):
        if up:
            return jnp.logical_and(z - k >= 0, z + 1 < nz)
        return jnp.logical_and(z + k < nz, z >= 1)

    def arrives(k, up):
        return (z - k >= 0) if up else (z + k < nz)

    for sub in range(SUBS):
        for up in (True, False):

            @pl.when(goes(0, up))
            def _():
                line(0, sub, up, True).start()

        h_copy(z, x, sub, side, h_side.at[0, sub, 0], True).start()
    for j in range(3):
        for o in range(1, ny):
            w_copy(d, j, far(o), w_far.at[o, j], True).start()
        w_copy(d, j, mate, w_near.at[0, j], True).start()

    h_all[pl.ds(pl.multiple_of(s * rows, rows), rows), :] = h_in[...]
    c_all[pl.ds(pl.multiple_of(s * rows, rows), rows), :] = c_in[
        :, pl.ds(pl.multiple_of(s * columns, columns), columns)
    ]
    for j, w in enumerate((wq, wk, wv)):
        w_all[pl.ds(pl.multiple_of(d * depth, depth), depth), j * columns : (j + 1) * columns] = w[...]

    def pass_weights(j):
        for o in range(1, ny):
            w_copy(far(o), j, mate, w_near.at[o, j]).wait_recv()
            w_copy(far(o), j, mate, w_near.at[o, j]).start()

    def send_cotangent():
        for hop in range(1, n):
            c_copy(hop).start()

    passed = 0
    for k in range(1, nz):
        for sub in range(SUBS):
            for up in (True, False):

                @pl.when(arrives(k, up))
                def _():
                    source = (z - k) if up else (z + k)
                    h_copy(source, x, sub, side, h_side.at[k, sub, int(up)]).wait_recv()
                    h_copy(source, x, sub, side, h_side.at[k, sub, int(up)]).start()

                @pl.when(goes(k, up))
                def _():
                    line(k, sub, up, False).start()

    send_cotangent()
    for j in range(passed, 3):
        pass_weights(j)

    for j in range(3):
        w_copy(mate, j, mate, w_near.at[0, j]).wait_recv()
        for o in range(1, ny):
            other = far(o) + 1 - 2 * core
            w_copy(other, j, mate, w_near.at[o, j]).wait_recv()

    @pl.loop(0, nz)
    def _(zz):
        project(zz * 2 + x)

    turn = 1 - 2 * (z // ((nz + 1) // 2))

    @pl.loop(0, nz)
    def _(k):
        zz = (z + turn * k + nz) % nz
        for sub in range(SUBS):
            h_copy(zz, 1 - x, sub, side, h_side.at[0, sub, 0]).wait_recv()
        project(zz * 2 + 1 - x)

    for k in range(1, n):
        c_copy(k).wait_recv()
    def drain():
        for k in range(1, n):
            c_copy(k).wait_send()
        for j in range(3):
            for o in range(ny):
                w_copy(d, j, mate, w_near.at[o, j]).wait_send()
                if o:
                    w_copy(d, j, far(o), w_far.at[o, j]).wait_send()
        for sub in range(SUBS):
            h_copy(z, x, sub, side, h_side.at[0, sub, 0]).wait_send()
            for up in (True, False):
                for k in range(nz):

                    @pl.when(goes(k, up))
                    def _():
                        line(k, sub, up, False).wait_send()

                    if k:

                        @pl.when(arrives(k, up))
                        def _():
                            h_copy(z, x, sub, side, h_side.at[k, sub, int(up)]).wait_send()

    return drain


def project_block(h_all, w_all, p_all, rows, columns, scale, block):
    at = pl.ds(pl.multiple_of(block * rows, rows), rows)
    for j in range(3):
        value = dot(h_all[at, :], w_all[:, j * columns : (j + 1) * columns]).astype(BF16)
        if j == 1:
            value = (value.astype(F32) * scale).astype(BF16)
        p_all[at, j * columns : (j + 1) * columns] = value


def mixer_phase(heads, rate, c_all, p_all, g_all, state, back):
    length, columns = c_all.shape
    dim = columns // heads
    blocks = length // BLOCK
    scale = dim ** (-0.5)
    row = lax.broadcasted_iota(jnp.int32, (BLOCK, BLOCK), 0).astype(F32)
    col = lax.broadcasted_iota(jnp.int32, (BLOCK, BLOCK), 1).astype(F32)
    place = lax.broadcasted_iota(jnp.int32, (BLOCK, dim), 0).astype(F32)
    spread = row - col
    state[...] = jnp.zeros_like(state)
    back[...] = jnp.zeros_like(back)

    @pl.loop(0, blocks)
    def _(i):
        for h in range(heads):
            g = rate[h]
            inner = jnp.where(spread >= 0, jnp.exp(g * jnp.maximum(spread, 0.0)), 0.0)
            inner_t = jnp.where(spread <= 0, jnp.exp(g * jnp.maximum(-spread, 0.0)), 0.0)
            query_decay = jnp.exp(g * (place + 1.0))
            key_decay = jnp.exp(g * (BLOCK - 1.0 - place))
            block_decay = jnp.exp(jnp.full((1, dim), g * BLOCK, F32))
            parts = [slice(j * columns + h * dim, j * columns + (h + 1) * dim) for j in range(3)]

            at = pl.ds(pl.multiple_of(i * BLOCK, BLOCK), BLOCK)
            k, v = p_all[at, parts[1]], p_all[at, parts[2]]
            c = c_all[at, parts[0]]
            mixed = (dot(c, v, NT) * inner).astype(BF16)
            held = state[h]
            grad_q = dot(mixed, k) + dot(c, held.astype(BF16), NT) * query_decay
            weighted = (k.astype(F32) * key_decay).astype(BF16)
            state[h] = held * block_decay + dot(weighted, v, TN)
            g_all[at, parts[0]] = grad_q.astype(BF16)

            at = pl.ds(pl.multiple_of((blocks - 1 - i) * BLOCK, BLOCK), BLOCK)
            q, k, v = (p_all[at, part] for part in parts)
            c = c_all[at, parts[0]]
            mixed_t = (dot(v, c, NT) * inner_t).astype(BF16)
            scores_t = (dot(k, q, NT) * inner_t).astype(BF16)
            held = back[h]
            held_bf = held.astype(BF16)
            grad_v = dot(scores_t, c) + dot(k, held_bf) * key_decay
            grad_k = (dot(mixed_t, q) + dot(v, held_bf, NT) * key_decay) * scale
            weighted = (q.astype(F32) * query_decay).astype(BF16)
            back[h] = held * block_decay + dot(weighted, c, TN)
            g_all[at, parts[1]] = grad_k.astype(BF16)
            g_all[at, parts[2]] = grad_v.astype(BF16)


def scatter_phase(
    n, m, h_all, w_all, g_all, dh, dq, dk, dv,
    part, ring, turned, near_out, near_in, far_out, far_in,
    r_send, r_recv, n_send, n_recv, f_send, f_recv,
):
    s = lax.axis_index("sp")
    d = lax.axis_index("dp")
    z, x = s // 2, s % 2
    y, core = d // 2, d % 2
    nz, ny = n // 2, m // 2
    rows, width = dh.shape
    depth, columns = dq.shape
    half = rows // 2
    sub_rows = half // SUBS
    mate = d + 1 - 2 * core
    me = x * (n - 1 - z) + (1 - x) * z

    def at_ring(p):
        p = (p + 2 * n) % n
        hi = p // nz
        return (hi * (n - 1 - p) + (1 - hi) * p) * 2 + hi

    def far(o):
        return ((y + o) % ny) * 2 + core

    right, left = at_ring(me + 1), at_ring(me - 1)

    def own(offset):
        return pl.multiple_of(at_ring(me + offset) * rows, rows)

    ready = set()

    def compute(*offsets):
        todo = []
        for offset in offsets:
            if offset % n not in ready:
                ready.add(offset % n)
                todo.append(own(offset))
        if not todo:
            return
        chunk = width // 4

        @pl.loop(0, 4)
        def _(i):
            at = pl.ds(pl.multiple_of(i * chunk, chunk), chunk)
            lhs = jnp.concatenate([g_all[pl.ds(base, rows), :] for base in todo], axis=0)
            value = dot(lhs, w_all[at, :], NT).astype(BF16)
            for spot, base in enumerate(todo):
                part[pl.ds(base, rows), at] = value[spot * rows : (spot + 1) * rows]

    def r_copy(step, way, sub):
        lane = (slice(0, half), slice(half, rows))[way].start + sub * sub_rows
        if step == 0:
            base = own(-1 if way == 0 else 1)
            src = part.at[pl.ds(pl.multiple_of(base + lane, sub_rows), sub_rows)]
        else:
            src = ring.at[step - 1, way, sub]
        return remote(
            src,
            ring.at[step, way, sub],
            r_send.at[step, way, sub],
            r_recv.at[step, way, sub],
            {"sp": right if way == 0 else left},
        )

    def process(step):
        for sub in range(SUBS):
            for way in range(2):
                base = own(-(step + 2) if way == 0 else step + 2)
                lane = way * half + sub * sub_rows
                r_copy(step, way, sub).wait_recv()
                mine = part[pl.ds(pl.multiple_of(base + lane, sub_rows), sub_rows), :]
                total = (ring[step, way, sub].astype(F32) + mine.astype(F32)).astype(BF16)
                if step < n - 2:
                    ring[step, way, sub] = total
                    r_copy(step + 1, way, sub).start()
                else:
                    dh[lane : lane + sub_rows, :] = total

    def turn(device):
        turned[...] = h_all[:, pl.ds(pl.multiple_of(device * depth, depth), depth)].T

    def weight_part(j):
        return dot(turned[...], g_all[:, pl.ds(pl.multiple_of(j * columns, columns), columns)])

    def n_copy(o):
        return remote(near_out.at[o], near_in.at[o], n_send.at[o], n_recv.at[o], {"dp": mate})

    def f_copy(o, j):
        return remote(
            far_out.at[o - 1, j], far_in.at[o - 1, j], f_send.at[o - 1, j], f_recv.at[o - 1, j], {"dp": far(o)}
        )

    def near(o):
        turn(far(o) + 1 - 2 * core)

        @pl.loop(0, 3)
        def _(j):
            near_out[o, j] = weight_part(j).astype(BF16)

        n_copy(o).start()

    def chip_sum(o):
        turn(far(o))
        n_copy(o).wait_recv()
        if o:
            for j in range(3):
                far_out[o - 1, j] = (weight_part(j) + near_in[o, j].astype(F32)).astype(BF16)
                f_copy(o, j).start()
        else:
            for j, out in enumerate((dq, dk, dv)):
                out[...] = weight_part(j) + near_in[o, j].astype(F32)

    tasks = []
    for o in range(1, ny):
        tasks += [functools.partial(near, o), functools.partial(chip_sum, o)]
    tasks += [functools.partial(near, 0), functools.partial(chip_sum, 0)]

    compute(-1, 1)
    for sub in range(SUBS):
        for way in range(2):
            r_copy(0, way, sub).start()
    for step in range(n - 1):
        early = step % 2 == 0
        if early and tasks:
            tasks.pop(0)()
        compute(-(step + 2), step + 2)
        process(step)
        if not early and tasks:
            tasks.pop(0)()
        if step == 0 and tasks:
            tasks.pop(0)()
        if step + 3 == n // 2:
            compute(n // 2, 0)
    while tasks:
        tasks.pop(0)()
    for j, out in enumerate((dq, dk, dv)):
        total = out[...]
        for o in range(1, ny):
            f_copy(o, j).wait_recv()
            total = total + far_in[o - 1, j].astype(F32)
        out[...] = total * (1.0 / m)
    for step in range(n - 1):
        for sub in range(SUBS):
            for way in range(2):
                r_copy(step, way, sub).wait_send()
    for o in range(ny):
        n_copy(o).wait_send()
        if o:
            for j in range(3):
                f_copy(o, j).wait_send()


def whole_kernel(n, m, heads, rate, h_in, c_in, wq, wk, wv, dh, dq, dk, dv, *scratch):
    h_all, c_all, w_all, p_all, g_all, state, back = scratch[:7]
    gather_sems, rest = scratch[7:15], scratch[15:]
    columns = wq.shape[1]
    project = functools.partial(
        project_block, h_all, w_all, p_all, h_in.shape[0], columns, (columns // heads) ** (-0.5)
    )
    drain = gather_phase(
        n, m, project, h_in, c_in, wq, wk, wv, h_all, c_all, w_all, *gather_sems
    )
    mixer_phase(heads, rate, c_all, p_all, g_all, state, back)
    scatter_phase(n, m, h_all, w_all, g_all, dh, dq, dk, dv, *rest)
    drain()


def whole(n, m, rate, h, c, wq, wk, wv):
    rows, width = h.shape
    depth, columns = wq.shape
    heads = rate.shape[0]
    dim = columns // heads
    length = rows * n
    ny = m // 2
    vmem = pl.BlockSpec(memory_space=pltpu.VMEM)
    dma = pltpu.SemaphoreType.DMA
    sub_rows = rows // 2 // SUBS
    return pl.pallas_call(
        functools.partial(whole_kernel, n, m, heads),
        out_shape=(pltpu.VMEM((rows, width), BF16),)
        + (pltpu.VMEM((depth, columns), F32),) * 3,
        in_specs=[pl.BlockSpec(memory_space=pltpu.SMEM)] + [vmem] * 5,
        out_specs=(vmem,) * 4,
        scratch_shapes=[
            pltpu.VMEM((length, width), BF16),
            pltpu.VMEM((length, columns), BF16),
            pltpu.VMEM((depth * m, 3 * columns), BF16),
            pltpu.VMEM((length, 3 * columns), BF16),
            pltpu.VMEM((length, 3 * columns), BF16),
            pltpu.VMEM((heads, dim, dim), F32),
            pltpu.VMEM((heads, dim, dim), F32),
            dma((n, SUBS)),
            dma((n // 2, SUBS, 2)),
            dma((n // 2, SUBS, 2)),
            dma((n - 1,)),
            dma((n - 1,)),
            dma((ny, 3)),
            dma((ny, 3)),
            dma((m, 3)),
            pltpu.VMEM((length, width), BF16),
            pltpu.VMEM((n - 1, 2, SUBS, sub_rows, width), BF16),
            pltpu.VMEM((depth, length), BF16),
            pltpu.VMEM((ny, 3, depth, columns), BF16),
            pltpu.VMEM((ny, 3, depth, columns), BF16),
            pltpu.VMEM((ny - 1, 3, depth, columns), BF16),
            pltpu.VMEM((ny - 1, 3, depth, columns), BF16),
            dma((n - 1, 2, SUBS)),
            dma((n - 1, 2, SUBS)),
            dma((ny,)),
            dma((ny,)),
            dma((ny - 1, 3)),
            dma((ny - 1, 3)),
        ],
        compiler_params=pltpu.CompilerParams(
            collective_id=0, has_side_effects=True, vmem_limit_bytes=VMEM_LIMIT
        ),
        name="whole",
    )(rate, h, c, wq, wk, wv)


def finish_kernel(count, *refs):
    ins, outs, sems = refs[:count], refs[count : 2 * count], refs[2 * count]
    moves = [pltpu.make_async_copy(ins[i], outs[i], sems.at[i]) for i in range(count)]
    for move in moves:
        move.start()
    for move in moves:
        move.wait()


def finish(*arrays):
    count = len(arrays)
    return pl.pallas_call(
        functools.partial(finish_kernel, count),
        out_shape=tuple(jax.ShapeDtypeStruct(a.shape, a.dtype) for a in arrays),
        in_specs=[pl.BlockSpec(memory_space=pltpu.VMEM)] * count,
        out_specs=(pl.BlockSpec(memory_space=pl.ANY),) * count,
        scratch_shapes=[pltpu.SemaphoreType.DMA((count,))],
        compiler_params=pltpu.CompilerParams(vmem_limit_bytes=4 * 1024 * 1024),
        name="finish",
    )(*arrays)


def body(n, m, hidden_in, mix_cotangent, query_weight, key_weight, value_weight, decay_log):
    dh, dq, dk, dv = finish(
        *whole(
            n, m, decay_log, hidden_in[0], mix_cotangent[0], query_weight, key_weight, value_weight
        )
    )
    return dh[None], dq, dk, dv


def solution(mesh):
    placed = (
        P("dp", "sp", None),
        P("dp", "sp", None),
        P("dp", "sp"),
        P("dp", "sp"),
        P("dp", "sp"),
        P("sp"),
    )
    return jax.shard_map(
        functools.partial(body, mesh.shape["sp"], mesh.shape["dp"]),
        mesh=mesh,
        in_specs=placed,
        out_specs=(P("dp", "sp", None), P("dp", "sp"), P("dp", "sp"), P("dp", "sp")),
        check_vma=False,
    )
```

profile of v0, /device:TPU:0, one launch (start us, length us, event | category | flops | bytes accessed | tf_op | source)
XLA Modules:
  0.0 123.5 jit_solution(72487931110630471)
XLA Ops:
  0.6 121.0 %whole.1 = (bf16[128,2048]{1,0:T(8,128)(2,1)S(1)}, f32[512,512]{1,0:T(8,128)S(1)}, f32[512,512]{1,0:T(8,128)S(1)}, f32[512,512]{1,0:T(8,128)S(1)}) custom-call(f32[2]{0:T(128)} %rate.1, bf16[128,2048]{1,0:T(8,128)(2,1)} %bitcast.4, bf16[128,4096]{1,0:T(8,128)(2,1)} %bitcast.3, bf16[512,512]{1,0:T(8,128)(2,1)} %wq.1, bf16[512,512]{1,0:T(8,128)(2,1)} %wk.1, ...), custom_call_target="tpu_custom_call" | custom-call | tf_op jit(solution)/shard_map/whole/pallas_call | solution.py:426
  121.6 1.9 %finish.1 = (bf16[128,2048]{1,0:T(8,128)(2,1)}, f32[512,512]{1,0:T(8,128)}, f32[512,512]{1,0:T(8,128)}, f32[512,512]{1,0:T(8,128)}) custom-call(bf16[128,2048]{1,0:T(8,128)(2,1)S(1)} %get-tuple-element.12.refs_0_, f32[512,512]{1,0:T(8,128)S(1)} %get-tuple-element.13.refs_1_, f32[512,512]{1,0:T(8,128)S(1)} %get-tuple-element.14.refs_2_, ...), custom_call_target="tpu_custom_call" | custom-call | tf_op jit(solution)/shard_map/finish/pallas_call | solution.py:480
where the time goes:
time: 124 us; the launch traced here: 123 us
  Pallas kernels  123 us (99%)
    pallas_call x1, Pallas kernels, whole(): pl.pallas_call(functools.partial(whole_kernel, n, m, heads), out_shape=(p...  121 us

commit v1 on v0

--- a/solution.py
+++ b/solution.py
@@ -9,6 +9,8 @@
 
 BLOCK = 128
 SUBS = 2
+CHUNKS = 4
+PIECES = 4
 F32 = jnp.float32
 BF16 = jnp.bfloat16
 MESH = pl.DeviceIdType.MESH
@@ -21,6 +23,10 @@
     return lax.dot_general(a, b, dims, preferred_element_type=F32)
 
 
+def scope(name, *tags):
+    return jax.named_scope("#".join([name] + [str(t) for t in tags]))
+
+
 def remote(src, dst, send, recv, where):
     return pltpu.make_async_remote_copy(
         src_ref=src, dst_ref=dst, send_sem=send, recv_sem=recv, device_id=where, device_id_type=MESH
@@ -31,11 +37,11 @@
     barrier = pltpu.get_barrier_semaphore()
     for where in targets:
         pl.semaphore_signal(barrier, inc=1, device_id=where, device_id_type=MESH)
-    pl.semaphore_wait(barrier, len(targets))
+    return lambda: pl.semaphore_wait(barrier, len(targets))
 
 
 def gather_phase(
-    n, m, project, h_in, c_in, wq, wk, wv, h_all, c_all, w_all,
+    n, m, project, h_in, c_in, wq, wk, wv, h_all, c_all, w_all, c_own, l_sem,
     h_recv, h_line, h_side, c_send, c_recv, w_far, w_near, w_recv,
 ):
     s = lax.axis_index("sp")
@@ -52,38 +58,49 @@
     def far(o):
         return ((y + o) % ny) * 2 + core
 
-    greet(
+    arrived = greet(
         [{"sp": (s + k) % n} for k in range(1, n)]
         + [{"dp": mate}]
         + [{"dp": far(o)} for o in range(1, ny)]
     )
 
-    def h_copy(src_z, src_x, sub, dest, send, own=False):
+    own_rows = pl.ds(pl.multiple_of(s * rows, rows), rows)
+    own_depth = pl.ds(pl.multiple_of(d * depth, depth), depth)
+    loads = [pltpu.make_async_copy(h_in, h_all.at[own_rows], l_sem.at[0])]
+    for j, w in enumerate((wq, wk, wv)):
+        place = w_all.at[own_depth, pl.ds(j * columns, columns)]
+        loads.append(pltpu.make_async_copy(w, place, l_sem.at[1 + j]))
+    loads.append(pltpu.make_async_copy(c_in, c_own, l_sem.at[4]))
+    mine = c_in.at[:, pl.ds(pl.multiple_of(s * columns, columns), columns)]
+    loads.append(pltpu.make_async_copy(mine, c_all.at[own_rows], l_sem.at[5]))
+    for load in loads:
+        load.start()
+
+    def h_copy(src_z, src_x, sub, dest, send):
         block = src_z * 2 + src_x
         place = pl.ds(pl.multiple_of(block * rows + sub * sub_rows, sub_rows), sub_rows)
-        src = h_in.at[pl.ds(sub * sub_rows, sub_rows)] if own else h_all.at[place]
-        return remote(src, h_all.at[place], send, h_recv.at[block, sub], {"sp": dest})
-
-    def w_copy(src_d, j, dest, send, own=False):
+        return remote(h_all.at[place], h_all.at[place], send, h_recv.at[block, sub], {"sp": dest})
+
+    def w_copy(src_d, j, dest, send):
         place = w_all.at[
             pl.ds(pl.multiple_of(src_d * depth, depth), depth), pl.ds(j * columns, columns)
         ]
-        return remote((wq, wk, wv)[j] if own else place, place, send, w_recv.at[src_d, j], {"dp": dest})
+        return remote(place, place, send, w_recv.at[src_d, j], {"dp": dest})
 
     def c_copy(k):
         to = (s + k) % n
         return remote(
-            c_in.at[:, pl.ds(pl.multiple_of(to * columns, columns), columns)],
+            c_own.at[:, pl.ds(pl.multiple_of(to * columns, columns), columns)],
             c_all.at[pl.ds(pl.multiple_of(s * rows, rows), rows)],
             c_send.at[k - 1],
             c_recv.at[k - 1],
             {"sp": to},
         )
 
-    def line(k, sub, up, own):
+    def line(k, sub, up):
         source = (z - k) if up else (z + k)
         dest = (s + 2) if up else (s - 2)
-        return h_copy(source, x, sub, dest, h_line.at[k, sub, int(up)], own)
+        return h_copy(source, x, sub, dest, h_line.at[k, sub, int(up)])
 
     def goes(k, up):
         if up:
@@ -93,29 +110,29 @@
     def arrives(k, up):
         return (z - k >= 0) if up else (z + k < nz)
 
+    with scope("greet"):
+        loads[0].wait()
+        arrived()
     for sub in range(SUBS):
         for up in (True, False):
 
             @pl.when(goes(0, up))
             def _():
-                line(0, sub, up, True).start()
-
-        h_copy(z, x, sub, side, h_side.at[0, sub, 0], True).start()
+                line(0, sub, up).start()
+
+        h_copy(z, x, sub, side, h_side.at[0, sub, 0]).start()
     for j in range(3):
+        loads[1 + j].wait()
         for o in range(1, ny):
-            w_copy(d, j, far(o), w_far.at[o, j], True).start()
-        w_copy(d, j, mate, w_near.at[0, j], True).start()
-
-    h_all[pl.ds(pl.multiple_of(s * rows, rows), rows), :] = h_in[...]
-    c_all[pl.ds(pl.multiple_of(s * rows, rows), rows), :] = c_in[
-        :, pl.ds(pl.multiple_of(s * columns, columns), columns)
-    ]
-    for j, w in enumerate((wq, wk, wv)):
-        w_all[pl.ds(pl.multiple_of(d * depth, depth), depth), j * columns : (j + 1) * columns] = w[...]
+            w_copy(d, j, far(o), w_far.at[o, j]).start()
+        w_copy(d, j, mate, w_near.at[0, j]).start()
+    loads[4].wait()
+    loads[5].wait()
 
     def pass_weights(j):
         for o in range(1, ny):
-            w_copy(far(o), j, mate, w_near.at[o, j]).wait_recv()
+            with scope("wfar", j):
+                w_copy(far(o), j, mate, w_near.at[o, j]).wait_recv()
             w_copy(far(o), j, mate, w_near.at[o, j]).start()
 
     def send_cotangent():
@@ -130,12 +147,13 @@
                 @pl.when(arrives(k, up))
                 def _():
                     source = (z - k) if up else (z + k)
-                    h_copy(source, x, sub, side, h_side.at[k, sub, int(up)]).wait_recv()
+                    with scope("hline", k, sub, up):
+                        h_copy(source, x, sub, side, h_side.at[k, sub, int(up)]).wait_recv()
                     h_copy(source, x, sub, side, h_side.at[k, sub, int(up)]).start()
 
                 @pl.when(goes(k, up))
                 def _():
-                    line(k, sub, up, False).start()
+                    line(k, sub, up).start()
 
     send_cotangent()
     for j in range(passed, 3):
@@ -145,23 +163,29 @@
         w_copy(mate, j, mate, w_near.at[0, j]).wait_recv()
         for o in range(1, ny):
             other = far(o) + 1 - 2 * core
-            w_copy(other, j, mate, w_near.at[o, j]).wait_recv()
+            with scope("wmate", j):
+                w_copy(other, j, mate, w_near.at[o, j]).wait_recv()
 
     @pl.loop(0, nz)
     def _(zz):
-        project(zz * 2 + x)
+        with scope("projown"):
+            project(zz * 2 + x)
 
     turn = 1 - 2 * (z // ((nz + 1) // 2))
 
     @pl.loop(0, nz)
     def _(k):
         zz = (z + turn * k + nz) % nz
-        for sub in range(SUBS):
-            h_copy(zz, 1 - x, sub, side, h_side.at[0, sub, 0]).wait_recv()
-        project(zz * 2 + 1 - x)
-
-    for k in range(1, n):
-        c_copy(k).wait_recv()
+        with scope("sidewait"):
+            for sub in range(SUBS):
+                h_copy(zz, 1 - x, sub, side, h_side.at[0, sub, 0]).wait_recv()
+        with scope("projside"):
+            project(zz * 2 + 1 - x)
+
+    with scope("cwait"):
+        for k in range(1, n):
+            c_copy(k).wait_recv()
+
     def drain():
         for k in range(1, n):
             c_copy(k).wait_send()
@@ -177,7 +201,7 @@
 
                     @pl.when(goes(k, up))
                     def _():
-                        line(k, sub, up, False).wait_send()
+                        line(k, sub, up).wait_send()
 
                     if k:
 
@@ -257,8 +281,8 @@
     nz, ny = n // 2, m // 2
     rows, width = dh.shape
     depth, columns = dq.shape
-    half = rows // 2
-    sub_rows = half // SUBS
+    chunk = width // CHUNKS
+    lanes = rows // 2
     mate = d + 1 - 2 * core
     me = x * (n - 1 - z) + (1 - x) * z
 
@@ -277,130 +301,145 @@
 
     ready = set()
 
-    def compute(*offsets):
-        todo = []
-        for offset in offsets:
-            if offset % n not in ready:
-                ready.add(offset % n)
-                todo.append(own(offset))
+    def partial(q, *offsets):
+        todo = [o % n for o in offsets if (q, o % n) not in ready]
         if not todo:
             return
-        chunk = width // 4
-
-        @pl.loop(0, 4)
-        def _(i):
-            at = pl.ds(pl.multiple_of(i * chunk, chunk), chunk)
-            lhs = jnp.concatenate([g_all[pl.ds(base, rows), :] for base in todo], axis=0)
-            value = dot(lhs, w_all[at, :], NT).astype(BF16)
-            for spot, base in enumerate(todo):
-                part[pl.ds(base, rows), at] = value[spot * rows : (spot + 1) * rows]
-
-    def r_copy(step, way, sub):
-        lane = (slice(0, half), slice(half, rows))[way].start + sub * sub_rows
+        ready.update((q, o) for o in todo)
+        bases = [own(o) for o in todo]
+        with scope("partial", q, *todo):
+            lhs = jnp.concatenate([g_all[pl.ds(base, rows), :] for base in bases], axis=0)
+            value = dot(lhs, w_all[q * chunk : (q + 1) * chunk, :], NT).astype(BF16)
+            for place, base in enumerate(bases):
+                part[q, pl.ds(base, rows), :] = value[place * rows : (place + 1) * rows]
+
+    def spot(way, piece):
+        return way * (CHUNKS // 2) + piece // 2, (piece % 2) * lanes
+
+    def r_copy(step, way, piece):
+        q, lane = spot(way, piece)
         if step == 0:
             base = own(-1 if way == 0 else 1)
-            src = part.at[pl.ds(pl.multiple_of(base + lane, sub_rows), sub_rows)]
+            src = part.at[q, pl.ds(pl.multiple_of(base + lane, lanes), lanes)]
         else:
-            src = ring.at[step - 1, way, sub]
+            src = ring.at[step - 1, way, piece]
         return remote(
             src,
-            ring.at[step, way, sub],
-            r_send.at[step, way, sub],
-            r_recv.at[step, way, sub],
+            ring.at[step, way, piece],
+            r_send.at[step, way, piece],
+            r_recv.at[step, way, piece],
             {"sp": right if way == 0 else left},
         )
 
-    def process(step):
-        for sub in range(SUBS):
-            for way in range(2):
-                base = own(-(step + 2) if way == 0 else step + 2)
-                lane = way * half + sub * sub_rows
-                r_copy(step, way, sub).wait_recv()
-                mine = part[pl.ds(pl.multiple_of(base + lane, sub_rows), sub_rows), :]
-                total = (ring[step, way, sub].astype(F32) + mine.astype(F32)).astype(BF16)
-                if step < n - 2:
-                    ring[step, way, sub] = total
-                    r_copy(step + 1, way, sub).start()
-                else:
-                    dh[lane : lane + sub_rows, :] = total
-
-    def turn(device):
-        turned[...] = h_all[:, pl.ds(pl.multiple_of(device * depth, depth), depth)].T
-
-    def weight_part(j):
-        return dot(turned[...], g_all[:, pl.ds(pl.multiple_of(j * columns, columns), columns)])
-
-    def n_copy(o):
-        return remote(near_out.at[o], near_in.at[o], n_send.at[o], n_recv.at[o], {"dp": mate})
+    def process(step, piece):
+        for way in range(2):
+            offset = -(step + 2) if way == 0 else step + 2
+            q, lane = spot(way, piece)
+            partial(q, -(step + 2), step + 2)
+            with scope("ring", step, way, piece):
+                r_copy(step, way, piece).wait_recv()
+            mine = part[q, pl.ds(pl.multiple_of(own(offset) + lane, lanes), lanes), :]
+            total = (ring[step, way, piece].astype(F32) + mine.astype(F32)).astype(BF16)
+            if step < n - 2:
+                ring[step, way, piece] = total
+                r_copy(step + 1, way, piece).start()
+            else:
+                dh[lane : lane + lanes, q * chunk : (q + 1) * chunk] = total
+
+    def turn(slot, device):
+        turned[slot] = h_all[:, pl.ds(pl.multiple_of(device * depth, depth), depth)].T
+
+    def weight_part(slot, j):
+        return dot(turned[slot], g_all[:, j * columns : (j + 1) * columns])
+
+    def n_copy(o, j):
+        return remote(
+            near_out.at[o, j], near_in.at[o, j], n_send.at[o, j], n_recv.at[o, j], {"dp": mate}
+        )
 
     def f_copy(o, j):
         return remote(
             far_out.at[o - 1, j], far_in.at[o - 1, j], f_send.at[o - 1, j], f_recv.at[o - 1, j], {"dp": far(o)}
         )
 
-    def near(o):
-        turn(far(o) + 1 - 2 * core)
-
-        @pl.loop(0, 3)
-        def _(j):
-            near_out[o, j] = weight_part(j).astype(BF16)
-
-        n_copy(o).start()
-
-    def chip_sum(o):
-        turn(far(o))
-        n_copy(o).wait_recv()
+    def near(o, j):
+        if j == 0:
+            turn(0, far(o) + 1 - 2 * core)
+        with scope("near", o, j):
+            near_out[o, j] = weight_part(0, j).astype(BF16)
+        n_copy(o, j).start()
+
+    def chip_sum(o, j):
+        if j == 0:
+            turn(1, far(o))
+        with scope("chip_sum", o, j):
+            value = weight_part(1, j)
+            n_copy(o, j).wait_recv()
+            value = value + near_in[o, j].astype(F32)
         if o:
-            for j in range(3):
-                far_out[o - 1, j] = (weight_part(j) + near_in[o, j].astype(F32)).astype(BF16)
-                f_copy(o, j).start()
+            far_out[o - 1, j] = value.astype(BF16)
+            f_copy(o, j).start()
         else:
-            for j, out in enumerate((dq, dk, dv)):
-                out[...] = weight_part(j) + near_in[o, j].astype(F32)
+            (dq, dk, dv)[j][...] = value
+
+    def weight(kind, o, j):
+        return functools.partial(kind, o, j)
 
     tasks = []
-    for o in range(1, ny):
-        tasks += [functools.partial(near, o), functools.partial(chip_sum, o)]
-    tasks += [functools.partial(near, 0), functools.partial(chip_sum, 0)]
-
-    compute(-1, 1)
-    for sub in range(SUBS):
-        for way in range(2):
-            r_copy(0, way, sub).start()
+    for o in list(range(1, ny)) + [0]:
+        tasks += [weight(near, o, 0), weight(near, o, 1), weight(chip_sum, o, 0)]
+        tasks += [weight(near, o, 2), weight(chip_sum, o, 1), weight(chip_sum, o, 2)]
+
+    def work(count=1):
+        for _ in range(count):
+            if tasks:
+                tasks.pop(0)()
+
+    order = [q for k in range(CHUNKS // 2) for q in (k, CHUNKS // 2 + k)]
+    for q in order:
+        partial(q, -1, 1)
+        way, first = divmod(q, CHUNKS // 2)
+        for piece in (2 * first, 2 * first + 1):
+            r_copy(0, way, piece).start()
+    work()
+    for q in order[:2]:
+        partial(q, -2, 2)
+    work(2)
+    pairs = [(q, pair) for pair in [(-2, 2), (-3, 3), (n // 2, 0)] for q in order]
     for step in range(n - 1):
-        early = step % 2 == 0
-        if early and tasks:
-            tasks.pop(0)()
-        compute(-(step + 2), step + 2)
-        process(step)
-        if not early and tasks:
-            tasks.pop(0)()
-        if step == 0 and tasks:
-            tasks.pop(0)()
-        if step + 3 == n // 2:
-            compute(n // 2, 0)
-    while tasks:
-        tasks.pop(0)()
+        for piece in range(PIECES):
+            process(step, piece)
+            while pairs and all((pairs[0][0], o % n) in ready for o in pairs[0][1]):
+                pairs.pop(0)
+            if pairs and (step < 2 or not tasks):
+                q, pair = pairs.pop(0)
+                partial(q, *pair)
+                if step and piece % 2:
+                    work()
+            else:
+                work()
+    work(len(tasks))
     for j, out in enumerate((dq, dk, dv)):
         total = out[...]
         for o in range(1, ny):
-            f_copy(o, j).wait_recv()
+            with scope("fwait", o, j):
+                f_copy(o, j).wait_recv()
             total = total + far_in[o - 1, j].astype(F32)
         out[...] = total * (1.0 / m)
     for step in range(n - 1):
-        for sub in range(SUBS):
+        for piece in range(PIECES):
             for way in range(2):
-                r_copy(step, way, sub).wait_send()
+                r_copy(step, way, piece).wait_send()
     for o in range(ny):
-        n_copy(o).wait_send()
-        if o:
-            for j in range(3):
+        for j in range(3):
+            n_copy(o, j).wait_send()
+            if o:
                 f_copy(o, j).wait_send()
 
 
 def whole_kernel(n, m, heads, rate, h_in, c_in, wq, wk, wv, dh, dq, dk, dv, *scratch):
     h_all, c_all, w_all, p_all, g_all, state, back = scratch[:7]
-    gather_sems, rest = scratch[7:15], scratch[15:]
+    gather_sems, rest = scratch[7:17], scratch[17:]
     columns = wq.shape[1]
     project = functools.partial(
         project_block, h_all, w_all, p_all, h_in.shape[0], columns, (columns // heads) ** (-0.5)
@@ -408,9 +447,11 @@
     drain = gather_phase(
         n, m, project, h_in, c_in, wq, wk, wv, h_all, c_all, w_all, *gather_sems
     )
-    mixer_phase(heads, rate, c_all, p_all, g_all, state, back)
+    with scope("mixer"):
+        mixer_phase(heads, rate, c_all, p_all, g_all, state, back)
     scatter_phase(n, m, h_all, w_all, g_all, dh, dq, dk, dv, *rest)
-    drain()
+    with scope("drain"):
+        drain()
 
 
 def whole(n, m, rate, h, c, wq, wk, wv):
@@ -422,12 +463,12 @@
     ny = m // 2
     vmem = pl.BlockSpec(memory_space=pltpu.VMEM)
     dma = pltpu.SemaphoreType.DMA
-    sub_rows = rows // 2 // SUBS
     return pl.pallas_call(
         functools.partial(whole_kernel, n, m, heads),
         out_shape=(pltpu.VMEM((rows, width), BF16),)
         + (pltpu.VMEM((depth, columns), F32),) * 3,
-        in_specs=[pl.BlockSpec(memory_space=pltpu.SMEM)] + [vmem] * 5,
+        in_specs=[pl.BlockSpec(memory_space=pltpu.SMEM)]
+        + [pl.BlockSpec(memory_space=pl.ANY)] * 5,
         out_specs=(vmem,) * 4,
         scratch_shapes=[
             pltpu.VMEM((length, width), BF16),
@@ -437,6 +478,8 @@
             pltpu.VMEM((length, 3 * columns), BF16),
             pltpu.VMEM((heads, dim, dim), F32),
             pltpu.VMEM((heads, dim, dim), F32),
+            pltpu.VMEM((rows, columns * n), BF16),
+            dma((6,)),
             dma((n, SUBS)),
             dma((n // 2, SUBS, 2)),
             dma((n // 2, SUBS, 2)),
@@ -445,17 +488,17 @@
             dma((ny, 3)),
             dma((ny, 3)),
             dma((m, 3)),
-            pltpu.VMEM((length, width), BF16),
-            pltpu.VMEM((n - 1, 2, SUBS, sub_rows, width), BF16),
-            pltpu.VMEM((depth, length), BF16),
+            pltpu.VMEM((CHUNKS, length, width // CHUNKS), BF16),
+            pltpu.VMEM((n - 1, 2, PIECES, rows // 2, width // CHUNKS), BF16),
+            pltpu.VMEM((2, depth, length), BF16),
             pltpu.VMEM((ny, 3, depth, columns), BF16),
             pltpu.VMEM((ny, 3, depth, columns), BF16),
             pltpu.VMEM((ny - 1, 3, depth, columns), BF16),
             pltpu.VMEM((ny - 1, 3, depth, columns), BF16),
-            dma((n - 1, 2, SUBS)),
-            dma((n - 1, 2, SUBS)),
-            dma((ny,)),
-            dma((ny,)),
+            dma((n - 1, 2, PIECES)),
+            dma((n - 1, 2, PIECES)),
+            dma((ny, 3)),
+            dma((ny, 3)),
             dma((ny - 1, 3)),
             dma((ny - 1, 3)),
         ],

time: 124 us -> 118 us (0.952)
  Pallas kernels: 123 us -> 117 us
    pallas_call x1, Pallas kernels: 121 us -> 115 us  [whole(): pl.pallas_call(functools.partial(whole_kernel, n, m, heads), out_shape=(p...]
where the time goes in v1:
time: 118 us
  Pallas kernels  117 us (99%)
    pallas_call x1, Pallas kernels, whole(): pl.pallas_call(functools.partial(whole_kernel, n, m, heads), out_shape=(p...  115 us

profile of v1, /device:TPU:0, one launch (start us, length us, event | category | flops | bytes accessed | tf_op | source)
XLA Modules:
  0.0 118.1 jit_solution(14370809046999268583)
XLA Ops:
  0.6 115.4 %whole.1 = (bf16[128,2048]{1,0:T(8,128)(2,1)S(1)}, f32[512,512]{1,0:T(8,128)S(1)}, f32[512,512]{1,0:T(8,128)S(1)}, f32[512,512]{1,0:T(8,128)S(1)}) custom-call(f32[2]{0:T(128)} %rate.1, bf16[128,2048]{1,0:T(8,128)(2,1)} %bitcast.4, bf16[128,4096]{1,0:T(8,128)(2,1)} %bitcast.3, bf16[512,512]{1,0:T(8,128)(2,1)} %wq.1, bf16[512,512]{1,0:T(8,128)(2,1)} %wk.1, ...), custom_call_target="tpu_custom_call" | custom-call | tf_op jit(solution)/shard_map/whole/pallas_call | solution.py:466
  116.0 1.9 %finish.1 = (bf16[128,2048]{1,0:T(8,128)(2,1)}, f32[512,512]{1,0:T(8,128)}, f32[512,512]{1,0:T(8,128)}, f32[512,512]{1,0:T(8,128)}) custom-call(bf16[128,2048]{1,0:T(8,128)(2,1)S(1)} %get-tuple-element.12.refs_0_, f32[512,512]{1,0:T(8,128)S(1)} %get-tuple-element.13.refs_1_, f32[512,512]{1,0:T(8,128)S(1)} %get-tuple-element.14.refs_2_, ...), custom_call_target="tpu_custom_call" | custom-call | tf_op jit(solution)/shard_map/finish/pallas_call | solution.py:523

commit v2 on v1

--- a/solution.py
+++ b/solution.py
@@ -16,7 +16,7 @@
 MESH = pl.DeviceIdType.MESH
 NT = (((1,), (1,)), ((), ()))
 TN = (((0,), (0,)), ((), ()))
-VMEM_LIMIT = 52 * 1024 * 1024
+VMEM_LIMIT = 58 * 1024 * 1024
 
 
 def dot(a, b, dims=(((1,), (0,)), ((), ()))):
@@ -33,16 +33,24 @@
     )
 
 
-def greet(targets):
+def greet(always, sometimes):
     barrier = pltpu.get_barrier_semaphore()
-    for where in targets:
+    count = len(always)
+    for where in always:
         pl.semaphore_signal(barrier, inc=1, device_id=where, device_id_type=MESH)
-    return lambda: pl.semaphore_wait(barrier, len(targets))
+    for there, where in sometimes:
+        count = count + jnp.where(there, 1, 0)
+
+        @pl.when(there)
+        def _():
+            pl.semaphore_signal(barrier, inc=1, device_id=where, device_id_type=MESH)
+
+    return lambda: pl.semaphore_wait(barrier, count)
 
 
 def gather_phase(
-    n, m, project, h_in, c_in, wq, wk, wv, h_all, c_all, w_all, c_own, l_sem,
-    h_recv, h_line, h_side, c_send, c_recv, w_far, w_near, w_recv,
+    n, m, project, local, tables, h_in, c_in, wq, wk, wv, h_all, c_all, w_all, c_own, c_via, l_sem,
+    h_recv, h_line, h_side, h_bridge, c_send, c_recv, v_send, v_recv, w_far, w_near, w_recv,
 ):
     s = lax.axis_index("sp")
     d = lax.axis_index("dp")
@@ -54,25 +62,33 @@
     depth, columns = wq.shape
     side = s + 1 - 2 * x
     mate = d + 1 - 2 * core
+    bridged = nz > 2
+    is_end = jnp.logical_or(z == 0, z == nz - 1)
+    inner = jnp.logical_not(is_end)
+    inward = jnp.where(z == 0, s + 2, s - 2)
 
     def far(o):
         return ((y + o) % ny) * 2 + core
 
     arrived = greet(
-        [{"sp": (s + k) % n} for k in range(1, n)]
-        + [{"dp": mate}]
-        + [{"dp": far(o)} for o in range(1, ny)]
+        [{"sp": side}, {"dp": mate}] + [{"dp": far(o)} for o in range(1, ny)],
+        [(z >= 1, {"sp": s - 2}), (z + 1 < nz, {"sp": s + 2})],
     )
 
-    own_rows = pl.ds(pl.multiple_of(s * rows, rows), rows)
+    def part_rows(block):
+        return pl.ds(pl.multiple_of(block * rows, rows), rows)
+
+    def part_columns(block):
+        return pl.ds(pl.multiple_of(block * columns, columns), columns)
+
     own_depth = pl.ds(pl.multiple_of(d * depth, depth), depth)
-    loads = [pltpu.make_async_copy(h_in, h_all.at[own_rows], l_sem.at[0])]
+    loads = [pltpu.make_async_copy(h_in, h_all.at[part_rows(s)], l_sem.at[0])]
     for j, w in enumerate((wq, wk, wv)):
         place = w_all.at[own_depth, pl.ds(j * columns, columns)]
         loads.append(pltpu.make_async_copy(w, place, l_sem.at[1 + j]))
     loads.append(pltpu.make_async_copy(c_in, c_own, l_sem.at[4]))
-    mine = c_in.at[:, pl.ds(pl.multiple_of(s * columns, columns), columns)]
-    loads.append(pltpu.make_async_copy(mine, c_all.at[own_rows], l_sem.at[5]))
+    mine = c_in.at[:, part_columns(s)]
+    loads.append(pltpu.make_async_copy(mine, c_all.at[part_rows(s)], l_sem.at[5]))
     for load in loads:
         load.start()
 
@@ -87,14 +103,28 @@
         ]
         return remote(place, place, send, w_recv.at[src_d, j], {"dp": dest})
 
-    def c_copy(k):
-        to = (s + k) % n
+    def c_copy(to):
         return remote(
-            c_own.at[:, pl.ds(pl.multiple_of(to * columns, columns), columns)],
-            c_all.at[pl.ds(pl.multiple_of(s * rows, rows), rows)],
-            c_send.at[k - 1],
-            c_recv.at[k - 1],
-            {"sp": to},
+            c_own.at[:, part_columns(to)], c_all.at[part_rows(s)], c_send.at[to], c_recv.at[s], {"sp": to}
+        )
+
+    def c_arrival(block):
+        return remote(
+            c_all.at[part_rows(block)], c_all.at[part_rows(block)], c_send.at[block], c_recv.at[block], {"sp": side}
+        )
+
+    def end_block(e, column):
+        return e * (nz - 1) * 2 + column
+
+    def c_cross(e):
+        to = end_block(e, 1 - x)
+        return remote(
+            c_own.at[:, part_columns(to)], c_via.at[e], c_send.at[to], v_recv.at[e], {"sp": side}
+        )
+
+    def c_pass(e):
+        return remote(
+            c_via.at[e], c_all.at[part_rows(side)], v_send.at[e], c_recv.at[side], {"sp": end_block(e, x)}
         )
 
     def line(k, sub, up):
@@ -109,6 +139,15 @@
 
     def arrives(k, up):
         return (z - k >= 0) if up else (z + k < nz)
+
+    def crosses(k, up):
+        here = arrives(k, up)
+        if not bridged or k != 1:
+            return here
+        return jnp.logical_and(here, (z != 1) if up else (z != nz - 2))
+
+    def bridge(sub):
+        return h_copy(z, 1 - x, sub, inward, h_bridge.at[sub])
 
     with scope("greet"):
         loads[0].wait()
@@ -128,6 +167,14 @@
         w_copy(d, j, mate, w_near.at[0, j]).start()
     loads[4].wait()
     loads[5].wait()
+    if bridged:
+
+        @pl.when(inner)
+        def _():
+            for e in range(2):
+                c_cross(e).start()
+
+    tables()
 
     def pass_weights(j):
         for o in range(1, ny):
@@ -135,12 +182,43 @@
                 w_copy(far(o), j, mate, w_near.at[o, j]).wait_recv()
             w_copy(far(o), j, mate, w_near.at[o, j]).start()
 
-    def send_cotangent():
-        for hop in range(1, n):
-            c_copy(hop).start()
+    def send_level(k, columns_too):
+        for up in (True, False):
+            to_z = (z + k) if up else (z - k)
+
+            @pl.when((to_z < nz) if up else (to_z >= 0))
+            def _():
+                c_copy(to_z * 2 + x).start()
+                if columns_too:
+                    c_copy(to_z * 2 + 1 - x).start()
+
+    def send_inner():
+        c_copy(side).start()
+        for k in range(1, nz):
+            for up in (True, False):
+                to_z = (z + k) if up else (z - k)
+
+                @pl.when((to_z < nz) if up else (to_z >= 0))
+                def _():
+                    c_copy(to_z * 2 + x).start()
+
+                @pl.when((to_z < nz - 1) if up else (to_z >= 1))
+                def _():
+                    c_copy(to_z * 2 + 1 - x).start()
+
+                @pl.when(to_z == (nz - 1 if up else 0))
+                def _():
+                    c_cross(int(up)).wait_recv()
+                    c_pass(int(up)).start()
 
     passed = 0
     for k in range(1, nz):
+        if bridged and k == nz - 1:
+
+            @pl.when(inner)
+            def _():
+                send_inner()
+
         for sub in range(SUBS):
             for up in (True, False):
 
@@ -149,13 +227,39 @@
                     source = (z - k) if up else (z + k)
                     with scope("hline", k, sub, up):
                         h_copy(source, x, sub, side, h_side.at[k, sub, int(up)]).wait_recv()
+
+                @pl.when(crosses(k, up))
+                def _():
+                    source = (z - k) if up else (z + k)
                     h_copy(source, x, sub, side, h_side.at[k, sub, int(up)]).start()
 
                 @pl.when(goes(k, up))
                 def _():
                     line(k, sub, up).start()
 
-    send_cotangent()
+            if bridged and k == 1:
+
+                @pl.when(is_end)
+                def _():
+                    h_copy(z, 1 - x, sub, side, h_side.at[0, sub, 0]).wait_recv()
+                    bridge(sub).start()
+
+            if bridged and (k, sub) in ((nz - 2, 0), (nz - 2, SUBS - 1), (nz - 1, 0)):
+                pass_weights(passed)
+                passed += 1
+        if bridged:
+
+            @pl.when(is_end)
+            def _():
+                if k == 1:
+                    c_copy(side).start()
+                send_level(k, True)
+
+    if not bridged:
+        c_copy(side).start()
+        for k in range(1, nz):
+            send_level(k, True)
+
     for j in range(passed, 3):
         pass_weights(j)
 
@@ -166,34 +270,73 @@
             with scope("wmate", j):
                 w_copy(other, j, mate, w_near.at[o, j]).wait_recv()
 
+    turn = 1 - 2 * (z // ((nz + 1) // 2))
+
+    def level(k):
+        return (z + turn * k + nz) % nz
+
+    def project_side(zz):
+        fresh = jnp.logical_not(jnp.logical_and(is_end, zz == z)) if bridged else True
+        with scope("sidewait"):
+
+            @pl.when(fresh)
+            def _():
+                for sub in range(SUBS):
+                    h_copy(zz, 1 - x, sub, side, h_side.at[0, sub, 0]).wait_recv()
+
+        with scope("projside"):
+            project(zz * 2 + 1 - x)
+
+    def mix(zz):
+        @pl.loop(0, 2)
+        def _(i):
+            block = zz * 2 + (x + i) % 2
+            with scope("cwait"):
+
+                @pl.when(block != s)
+                def _():
+                    c_arrival(block).wait_recv()
+
+            with scope("local"):
+                local(block)
+
     @pl.loop(0, nz)
     def _(zz):
         with scope("projown"):
             project(zz * 2 + x)
 
-    turn = 1 - 2 * (z // ((nz + 1) // 2))
+    @pl.loop(0, nz - 1)
+    def _(k):
+        project_side(level(k))
 
     @pl.loop(0, nz)
     def _(k):
-        zz = (z + turn * k + nz) % nz
-        with scope("sidewait"):
-            for sub in range(SUBS):
-                h_copy(zz, 1 - x, sub, side, h_side.at[0, sub, 0]).wait_recv()
-        with scope("projside"):
-            project(zz * 2 + 1 - x)
-
-    with scope("cwait"):
-        for k in range(1, n):
-            c_copy(k).wait_recv()
+        @pl.when(k == nz - 1)
+        def _():
+            project_side(level(k))
+
+        mix(level(k))
 
     def drain():
         for k in range(1, n):
-            c_copy(k).wait_send()
+            c_copy((s + k) % n).wait_send()
         for j in range(3):
             for o in range(ny):
                 w_copy(d, j, mate, w_near.at[o, j]).wait_send()
                 if o:
                     w_copy(d, j, far(o), w_far.at[o, j]).wait_send()
+        if bridged:
+
+            @pl.when(inner)
+            def _():
+                for e in range(2):
+                    c_pass(e).wait_send()
+
+            @pl.when(is_end)
+            def _():
+                for sub in range(SUBS):
+                    bridge(sub).wait_send()
+
         for sub in range(SUBS):
             h_copy(z, x, sub, side, h_side.at[0, sub, 0]).wait_send()
             for up in (True, False):
@@ -205,7 +348,7 @@
 
                     if k:
 
-                        @pl.when(arrives(k, up))
+                        @pl.when(crosses(k, up))
                         def _():
                             h_copy(z, x, sub, side, h_side.at[k, sub, int(up)]).wait_send()
 
@@ -221,52 +364,71 @@
         p_all[at, j * columns : (j + 1) * columns] = value
 
 
-def mixer_phase(heads, rate, c_all, p_all, g_all, state, back):
+def fill_tables(heads, rate, inner, inner_t, query_decay, key_decay):
+    dim = query_decay.shape[2]
+    row = lax.broadcasted_iota(jnp.int32, (BLOCK, BLOCK), 0).astype(F32)
+    col = lax.broadcasted_iota(jnp.int32, (BLOCK, BLOCK), 1).astype(F32)
+    place = lax.broadcasted_iota(jnp.int32, (BLOCK, dim), 0).astype(F32)
+    spread = row - col
+    for h in range(heads):
+        g = rate[h]
+        inner[h] = jnp.where(spread >= 0, jnp.exp(g * jnp.maximum(spread, 0.0)), 0.0)
+        inner_t[h] = jnp.where(spread <= 0, jnp.exp(g * jnp.maximum(-spread, 0.0)), 0.0)
+        query_decay[h] = jnp.exp(g * (place + 1.0))
+        key_decay[h] = jnp.exp(g * (BLOCK - 1.0 - place))
+
+
+def head_parts(columns, dim, h):
+    return [slice(j * columns + h * dim, j * columns + (h + 1) * dim) for j in range(3)]
+
+
+def local_block(heads, c_all, p_all, inner, inner_t, query_decay, key_decay, acc, s_term, r_term, block):
+    columns = c_all.shape[1]
+    dim = columns // heads
+    at = pl.ds(pl.multiple_of(block * BLOCK, BLOCK), BLOCK)
+    for h in range(heads):
+        parts = head_parts(columns, dim, h)
+        q, k, v = (p_all[at, part] for part in parts)
+        c = c_all[at, parts[0]]
+        mixed = (dot(c, v, NT) * inner[h]).astype(BF16)
+        mixed_t = (dot(v, c, NT) * inner_t[h]).astype(BF16)
+        scores_t = (dot(k, q, NT) * inner_t[h]).astype(BF16)
+        s_term[block, h] = dot((k.astype(F32) * key_decay[h]).astype(BF16), v, TN)
+        r_term[block, h] = dot((q.astype(F32) * query_decay[h]).astype(BF16), c, TN)
+        acc[at, parts[0]] = dot(mixed, k)
+        acc[at, parts[1]] = dot(mixed_t, q)
+        acc[at, parts[2]] = dot(scores_t, c)
+
+
+def chain_phase(heads, rate, c_all, p_all, g_all, query_decay, key_decay, acc, s_term, r_term, state, back):
     length, columns = c_all.shape
     dim = columns // heads
     blocks = length // BLOCK
     scale = dim ** (-0.5)
-    row = lax.broadcasted_iota(jnp.int32, (BLOCK, BLOCK), 0).astype(F32)
-    col = lax.broadcasted_iota(jnp.int32, (BLOCK, BLOCK), 1).astype(F32)
-    place = lax.broadcasted_iota(jnp.int32, (BLOCK, dim), 0).astype(F32)
-    spread = row - col
     state[...] = jnp.zeros_like(state)
     back[...] = jnp.zeros_like(back)
 
     @pl.loop(0, blocks)
     def _(i):
         for h in range(heads):
-            g = rate[h]
-            inner = jnp.where(spread >= 0, jnp.exp(g * jnp.maximum(spread, 0.0)), 0.0)
-            inner_t = jnp.where(spread <= 0, jnp.exp(g * jnp.maximum(-spread, 0.0)), 0.0)
-            query_decay = jnp.exp(g * (place + 1.0))
-            key_decay = jnp.exp(g * (BLOCK - 1.0 - place))
-            block_decay = jnp.exp(jnp.full((1, dim), g * BLOCK, F32))
-            parts = [slice(j * columns + h * dim, j * columns + (h + 1) * dim) for j in range(3)]
+            block_decay = jnp.exp(jnp.full((1, dim), rate[h] * BLOCK, F32))
+            parts = head_parts(columns, dim, h)
 
             at = pl.ds(pl.multiple_of(i * BLOCK, BLOCK), BLOCK)
-            k, v = p_all[at, parts[1]], p_all[at, parts[2]]
-            c = c_all[at, parts[0]]
-            mixed = (dot(c, v, NT) * inner).astype(BF16)
             held = state[h]
-            grad_q = dot(mixed, k) + dot(c, held.astype(BF16), NT) * query_decay
-            weighted = (k.astype(F32) * key_decay).astype(BF16)
-            state[h] = held * block_decay + dot(weighted, v, TN)
-            g_all[at, parts[0]] = grad_q.astype(BF16)
-
-            at = pl.ds(pl.multiple_of((blocks - 1 - i) * BLOCK, BLOCK), BLOCK)
-            q, k, v = (p_all[at, part] for part in parts)
-            c = c_all[at, parts[0]]
-            mixed_t = (dot(v, c, NT) * inner_t).astype(BF16)
-            scores_t = (dot(k, q, NT) * inner_t).astype(BF16)
+            across = dot(c_all[at, parts[0]], held.astype(BF16), NT) * query_decay[h]
+            g_all[at, parts[0]] = (acc[at, parts[0]] + across).astype(BF16)
+            state[h] = held * block_decay + s_term[i, h]
+
+            j = blocks - 1 - i
+            at = pl.ds(pl.multiple_of(j * BLOCK, BLOCK), BLOCK)
             held = back[h]
             held_bf = held.astype(BF16)
-            grad_v = dot(scores_t, c) + dot(k, held_bf) * key_decay
-            grad_k = (dot(mixed_t, q) + dot(v, held_bf, NT) * key_decay) * scale
-            weighted = (q.astype(F32) * query_decay).astype(BF16)
-            back[h] = held * block_decay + dot(weighted, c, TN)
-            g_all[at, parts[1]] = grad_k.astype(BF16)
-            g_all[at, parts[2]] = grad_v.astype(BF16)
+            across = dot(p_all[at, parts[2]], held_bf, NT) * key_decay[h]
+            g_all[at, parts[1]] = ((acc[at, parts[1]] + across) * scale).astype(BF16)
+            across = dot(p_all[at, parts[1]], held_bf) * key_decay[h]
+            g_all[at, parts[2]] = (acc[at, parts[2]] + across).astype(BF16)
+            back[h] = held * block_decay + r_term[j, h]
 
 
 def scatter_phase(
@@ -439,16 +601,19 @@
 
 def whole_kernel(n, m, heads, rate, h_in, c_in, wq, wk, wv, dh, dq, dk, dv, *scratch):
     h_all, c_all, w_all, p_all, g_all, state, back = scratch[:7]
-    gather_sems, rest = scratch[7:17], scratch[17:]
+    decays, (acc, s_term, r_term) = scratch[7:11], scratch[11:14]
+    gather_refs, rest = scratch[14:28], scratch[28:]
     columns = wq.shape[1]
     project = functools.partial(
         project_block, h_all, w_all, p_all, h_in.shape[0], columns, (columns // heads) ** (-0.5)
     )
+    local = functools.partial(local_block, heads, c_all, p_all, *decays, acc, s_term, r_term)
+    tables = functools.partial(fill_tables, heads, rate, *decays)
     drain = gather_phase(
-        n, m, project, h_in, c_in, wq, wk, wv, h_all, c_all, w_all, *gather_sems
+        n, m, project, local, tables, h_in, c_in, wq, wk, wv, h_all, c_all, w_all, *gather_refs
     )
-    with scope("mixer"):
-        mixer_phase(heads, rate, c_all, p_all, g_all, state, back)
+    with scope("chain"):
+        chain_phase(heads, rate, c_all, p_all, g_all, *decays[2:], acc, s_term, r_term, state, back)
     scatter_phase(n, m, h_all, w_all, g_all, dh, dq, dk, dv, *rest)
     with scope("drain"):
         drain()
@@ -478,13 +643,24 @@
             pltpu.VMEM((length, 3 * columns), BF16),
             pltpu.VMEM((heads, dim, dim), F32),
             pltpu.VMEM((heads, dim, dim), F32),
+            pltpu.VMEM((heads, BLOCK, BLOCK), F32),
+            pltpu.VMEM((heads, BLOCK, BLOCK), F32),
+            pltpu.VMEM((heads, BLOCK, dim), F32),
+            pltpu.VMEM((heads, BLOCK, dim), F32),
+            pltpu.VMEM((length, 3 * columns), F32),
+            pltpu.VMEM((length // BLOCK, heads, dim, dim), F32),
+            pltpu.VMEM((length // BLOCK, heads, dim, dim), F32),
             pltpu.VMEM((rows, columns * n), BF16),
+            pltpu.VMEM((2, rows, columns), BF16),
             dma((6,)),
             dma((n, SUBS)),
             dma((n // 2, SUBS, 2)),
             dma((n // 2, SUBS, 2)),
-            dma((n - 1,)),
-            dma((n - 1,)),
+            dma((SUBS,)),
+            dma((n,)),
+            dma((n,)),
+            dma((2,)),
+            dma((2,)),
             dma((ny, 3)),
             dma((ny, 3)),
             dma((m, 3)),

time: 118 us -> 112 us (0.949)
  Pallas kernels: 117 us -> 111 us
    pallas_call x1, Pallas kernels: 115 us -> 109 us  [whole(): pl.pallas_call(functools.partial(whole_kernel, n, m, heads), out_shape=(p...]
where the time goes in v2:
time: 112 us
  Pallas kernels  111 us (99%)
    pallas_call x1, Pallas kernels, whole(): pl.pallas_call(functools.partial(whole_kernel, n, m, heads), out_shape=(p...  109 us

profile of v2, /device:TPU:0, one launch (start us, length us, event | category | flops | bytes accessed | tf_op | source)
XLA Modules:
  0.0 111.5 jit_solution(11260260303352680682)
XLA Ops:
  0.6 108.8 %whole.1 = (bf16[128,2048]{1,0:T(8,128)(2,1)S(1)}, f32[512,512]{1,0:T(8,128)S(1)}, f32[512,512]{1,0:T(8,128)S(1)}, f32[512,512]{1,0:T(8,128)S(1)}) custom-call(f32[2]{0:T(128)} %rate.1, bf16[128,2048]{1,0:T(8,128)(2,1)} %bitcast.4, bf16[128,4096]{1,0:T(8,128)(2,1)} %bitcast.3, bf16[512,512]{1,0:T(8,128)(2,1)} %wq.1, bf16[512,512]{1,0:T(8,128)(2,1)} %wk.1, ...), custom_call_target="tpu_custom_call" | custom-call | tf_op jit(solution)/shard_map/whole/pallas_call | solution.py:631
  109.5 1.9 %finish.1 = (bf16[128,2048]{1,0:T(8,128)(2,1)}, f32[512,512]{1,0:T(8,128)}, f32[512,512]{1,0:T(8,128)}, f32[512,512]{1,0:T(8,128)}) custom-call(bf16[128,2048]{1,0:T(8,128)(2,1)S(1)} %get-tuple-element.12.refs_0_, f32[512,512]{1,0:T(8,128)S(1)} %get-tuple-element.13.refs_1_, f32[512,512]{1,0:T(8,128)S(1)} %get-tuple-element.14.refs_2_, ...), custom_call_target="tpu_custom_call" | custom-call | tf_op jit(solution)/shard_map/finish/pallas_call | solution.py:699

commit v3 on v2

--- a/solution.py
+++ b/solution.py
@@ -173,6 +173,7 @@
         def _():
             for e in range(2):
                 c_cross(e).start()
+            c_copy(side).start()
 
     tables()
 
@@ -182,34 +183,70 @@
                 w_copy(far(o), j, mate, w_near.at[o, j]).wait_recv()
             w_copy(far(o), j, mate, w_near.at[o, j]).start()
 
-    def send_level(k, columns_too):
+    def send_level(k):
         for up in (True, False):
             to_z = (z + k) if up else (z - k)
 
             @pl.when((to_z < nz) if up else (to_z >= 0))
             def _():
                 c_copy(to_z * 2 + x).start()
-                if columns_too:
-                    c_copy(to_z * 2 + 1 - x).start()
-
-    def send_inner():
-        c_copy(side).start()
-        for k in range(1, nz):
-            for up in (True, False):
-                to_z = (z + k) if up else (z - k)
-
-                @pl.when((to_z < nz) if up else (to_z >= 0))
-                def _():
-                    c_copy(to_z * 2 + x).start()
-
-                @pl.when((to_z < nz - 1) if up else (to_z >= 1))
-                def _():
-                    c_copy(to_z * 2 + 1 - x).start()
-
-                @pl.when(to_z == (nz - 1 if up else 0))
-                def _():
-                    c_cross(int(up)).wait_recv()
-                    c_pass(int(up)).start()
+                c_copy(to_z * 2 + 1 - x).start()
+
+    def send_column(k):
+        for up in (True, False):
+            to_z = (z + k) if up else (z - k)
+
+            @pl.when((to_z < nz) if up else (to_z >= 0))
+            def _():
+                c_copy(to_z * 2 + x).start()
+
+            @pl.when(to_z == (nz - 1 if up else 0))
+            def _():
+                c_cross(int(up)).wait_recv()
+                c_pass(int(up)).start()
+
+    def send_across(k):
+        for up in (True, False):
+            to_z = (z + k) if up else (z - k)
+
+            @pl.when((to_z < nz - 1) if up else (to_z >= 1))
+            def _():
+                c_copy(to_z * 2 + 1 - x).start()
+
+    upper = z // ((nz + 1) // 2)
+    from_low = upper * (nz - 1) + (1 - 2 * upper) * z
+
+    def level(k):
+        low = jnp.where(k == 0, from_low, jnp.where(k - 1 < from_low, k - 1, k))
+        return upper * (nz - 1) + (1 - 2 * upper) * low
+
+    def side_wait(zz):
+        fresh = jnp.logical_not(jnp.logical_and(is_end, zz == z)) if bridged else True
+        with scope("sidewait"):
+
+            @pl.when(fresh)
+            def _():
+                for sub in range(SUBS):
+                    h_copy(zz, 1 - x, sub, side, h_side.at[0, sub, 0]).wait_recv()
+
+    def wait_weights(j):
+        w_copy(mate, j, mate, w_near.at[0, j]).wait_recv()
+        for o in range(1, ny):
+            other = far(o) + 1 - 2 * core
+            with scope("wmate", j):
+                w_copy(other, j, mate, w_near.at[o, j]).wait_recv()
+
+    def early():
+        for j in range(2):
+            wait_weights(j)
+        with scope("early"):
+
+            @pl.loop(0, nz - 1)
+            def _(k):
+                project(level(k) * 2 + x, (0, 1))
+
+            side_wait(level(0))
+            project(level(0) * 2 + 1 - x, (0, 1))
 
     passed = 0
     for k in range(1, nz):
@@ -217,7 +254,7 @@
 
             @pl.when(inner)
             def _():
-                send_inner()
+                send_column(1)
 
         for sub in range(SUBS):
             for up in (True, False):
@@ -245,77 +282,85 @@
                     bridge(sub).start()
 
             if bridged and (k, sub) in ((nz - 2, 0), (nz - 2, SUBS - 1), (nz - 1, 0)):
+                if passed == 2:
+
+                    @pl.when(is_end)
+                    def _():
+                        for past in range(2, nz - 1):
+                            send_level(past)
+
+                    early()
                 pass_weights(passed)
                 passed += 1
-        if bridged:
+        if bridged and k == 1:
 
             @pl.when(is_end)
             def _():
-                if k == 1:
-                    c_copy(side).start()
-                send_level(k, True)
-
-    if not bridged:
+                c_copy(side).start()
+                send_level(1)
+
+    if bridged:
+
+        @pl.when(inner)
+        def _():
+            send_across(1)
+
+    else:
         c_copy(side).start()
         for k in range(1, nz):
-            send_level(k, True)
+            send_level(k)
 
     for j in range(passed, 3):
+        if j == 2:
+            early()
         pass_weights(j)
-
-    for j in range(3):
-        w_copy(mate, j, mate, w_near.at[0, j]).wait_recv()
-        for o in range(1, ny):
-            other = far(o) + 1 - 2 * core
-            with scope("wmate", j):
-                w_copy(other, j, mate, w_near.at[o, j]).wait_recv()
-
-    turn = 1 - 2 * (z // ((nz + 1) // 2))
-
-    def level(k):
-        return (z + turn * k + nz) % nz
-
-    def project_side(zz):
-        fresh = jnp.logical_not(jnp.logical_and(is_end, zz == z)) if bridged else True
-        with scope("sidewait"):
-
-            @pl.when(fresh)
-            def _():
-                for sub in range(SUBS):
-                    h_copy(zz, 1 - x, sub, side, h_side.at[0, sub, 0]).wait_recv()
-
-        with scope("projside"):
-            project(zz * 2 + 1 - x)
-
-    def mix(zz):
-        @pl.loop(0, 2)
-        def _(i):
-            block = zz * 2 + (x + i) % 2
-            with scope("cwait"):
-
-                @pl.when(block != s)
-                def _():
-                    c_arrival(block).wait_recv()
-
-            with scope("local"):
-                local(block)
-
-    @pl.loop(0, nz)
-    def _(zz):
-        with scope("projown"):
-            project(zz * 2 + x)
+    wait_weights(2)
+    if bridged:
+
+        @pl.when(inner)
+        def _():
+            for k in range(2, nz):
+                send_column(k)
+                send_across(k)
 
     @pl.loop(0, nz - 1)
     def _(k):
-        project_side(level(k))
-
-    @pl.loop(0, nz)
-    def _(k):
-        @pl.when(k == nz - 1)
+        project(level(k) * 2 + x, (2,))
+
+    project(level(0) * 2 + 1 - x, (2,))
+    project(level(nz - 1) * 2 + x, (0, 1, 2))
+
+    @pl.loop(0, 2 * nz - 1)
+    def _(t):
+        last = 2 * nz - 4
+        held = jnp.logical_and(t != last, jnp.logical_or(t == 0, t >= nz - 1))
+        mixes = jnp.where(is_end, held, t % 2 == 0)
+        late = jnp.where(t < nz - 1, t, jnp.where(t < last, t - nz + 2, t - nz + 1))
+        late = jnp.where(t == last, nz - 1, late)
+        zz = level(jnp.where(is_end, late, (t + 1) // 2))
+        if bridged:
+
+            @pl.when(jnp.logical_and(is_end, t == 1))
+            def _():
+                send_level(nz - 1)
+
+        @pl.when(jnp.logical_not(mixes))
         def _():
-            project_side(level(k))
-
-        mix(level(k))
+            side_wait(zz)
+            with scope("projside"):
+                project(zz * 2 + 1 - x, (0, 1, 2))
+
+        @pl.when(mixes)
+        def _():
+            with scope("cwait"):
+                for column in range(2):
+
+                    @pl.when(zz * 2 + column != s)
+                    def _():
+                        c_arrival(zz * 2 + column).wait_recv()
+
+            with scope("local"):
+                local(zz * 2, zz * 2 + 1)
 
     def drain():
         for k in range(1, n):
@@ -355,9 +400,9 @@
     return drain
 
 
-def project_block(h_all, w_all, p_all, rows, columns, scale, block):
+def project_block(h_all, w_all, p_all, rows, columns, scale, block, which):
     at = pl.ds(pl.multiple_of(block * rows, rows), rows)
-    for j in range(3):
+    for j in which:
         value = dot(h_all[at, :], w_all[:, j * columns : (j + 1) * columns]).astype(BF16)
         if j == 1:
             value = (value.astype(F32) * scale).astype(BF16)
@@ -382,11 +427,11 @@
     return [slice(j * columns + h * dim, j * columns + (h + 1) * dim) for j in range(3)]
 
 
-def local_block(heads, c_all, p_all, inner, inner_t, query_decay, key_decay, acc, s_term, r_term, block):
+def local_block(heads, c_all, p_all, inner, inner_t, query_decay, key_decay, acc, s_term, r_term, *blocks):
     columns = c_all.shape[1]
     dim = columns // heads
-    at = pl.ds(pl.multiple_of(block * BLOCK, BLOCK), BLOCK)
-    for h in range(heads):
+    for h, block in ((h, block) for h in range(heads) for block in blocks):
+        at = pl.ds(pl.multiple_of(block * BLOCK, BLOCK), BLOCK)
         parts = head_parts(columns, dim, h)
         q, k, v = (p_all[at, part] for part in parts)
         c = c_all[at, parts[0]]
@@ -408,20 +453,19 @@
     state[...] = jnp.zeros_like(state)
     back[...] = jnp.zeros_like(back)
 
-    @pl.loop(0, blocks)
-    def _(i):
+    for i in range(blocks):
         for h in range(heads):
             block_decay = jnp.exp(jnp.full((1, dim), rate[h] * BLOCK, F32))
             parts = head_parts(columns, dim, h)
 
-            at = pl.ds(pl.multiple_of(i * BLOCK, BLOCK), BLOCK)
+            at = slice(i * BLOCK, (i + 1) * BLOCK)
             held = state[h]
             across = dot(c_all[at, parts[0]], held.astype(BF16), NT) * query_decay[h]
             g_all[at, parts[0]] = (acc[at, parts[0]] + across).astype(BF16)
             state[h] = held * block_decay + s_term[i, h]
 
             j = blocks - 1 - i
-            at = pl.ds(pl.multiple_of(j * BLOCK, BLOCK), BLOCK)
+            at = slice(j * BLOCK, (j + 1) * BLOCK)
             held = back[h]
             held_bf = held.astype(BF16)
             across = dot(p_all[at, parts[2]], held_bf, NT) * key_decay[h]
@@ -432,7 +476,7 @@
 
 
 def scatter_phase(
-    n, m, h_all, w_all, g_all, dh, dq, dk, dv,
+    n, m, drain, h_all, w_all, g_all, dh, dq, dk, dv,
     part, ring, turned, near_out, near_in, far_out, far_in,
     r_send, r_recv, n_send, n_recv, f_send, f_recv,
 ):
@@ -488,7 +532,7 @@
         return remote(
             src,
             ring.at[step, way, piece],
-            r_send.at[step, way, piece],
+            r_send.at[step],
             r_recv.at[step, way, piece],
             {"sp": right if way == 0 else left},
         )
@@ -549,8 +593,9 @@
 
     tasks = []
     for o in list(range(1, ny)) + [0]:
-        tasks += [weight(near, o, 0), weight(near, o, 1), weight(chip_sum, o, 0)]
-        tasks += [weight(near, o, 2), weight(chip_sum, o, 1), weight(chip_sum, o, 2)]
+        first = [weight(near, o, 0), weight(chip_sum, o, 0)]
+        later = [weight(near, o, 1), weight(near, o, 2), weight(chip_sum, o, 1), weight(chip_sum, o, 2)]
+        tasks += first + later if o else [first[0], *later[:2], first[1], *later[2:]]
 
     def work(count=1):
         for _ in range(count):
@@ -558,18 +603,47 @@
                 tasks.pop(0)()
 
     order = [q for k in range(CHUNKS // 2) for q in (k, CHUNKS // 2 + k)]
-    for q in order:
+    for spot_in_order, q in enumerate(order):
+        if spot_in_order == 2:
+            work()
         partial(q, -1, 1)
         way, first = divmod(q, CHUNKS // 2)
         for piece in (2 * first, 2 * first + 1):
             r_copy(0, way, piece).start()
+    partial(order[0], -2, 2)
     work()
-    for q in order[:2]:
-        partial(q, -2, 2)
-    work(2)
+    partial(order[1], -2, 2)
+    work()
     pairs = [(q, pair) for pair in [(-2, 2), (-3, 3), (n // 2, 0)] for q in order]
+    def finish_weight(j):
+        out = (dq, dk, dv)[j]
+        total = out[...]
+        for o in range(1, ny):
+            with scope("fwait", o, j):
+                f_copy(o, j).wait_recv()
+            total = total + far_in[o - 1, j].astype(F32)
+        out[...] = total * (1.0 / m)
+        for o in range(1, ny):
+            f_copy(o, j).wait_send()
+
+    def sent(step):
+        pltpu.make_async_copy(ring.at[step], ring.at[step], r_send.at[step]).wait()
+
+    def settle():
+        for o in range(ny):
+            for j in range(3):
+                n_copy(o, j).wait_send()
+        drain()
+
     for step in range(n - 1):
         for piece in range(PIECES):
+            if step == n - 2 and piece != 2:
+                finish_weight(min(piece, 2))
+            if step > 1 and piece == 0:
+                sent(step - 2)
+            if step == n - 3 and piece == 0:
+                work(len(tasks))
+                settle()
             process(step, piece)
             while pairs and all((pairs[0][0], o % n) in ready for o in pairs[0][1]):
                 pairs.pop(0)
@@ -580,23 +654,9 @@
                     work()
             else:
                 work()
-    work(len(tasks))
-    for j, out in enumerate((dq, dk, dv)):
-        total = out[...]
-        for o in range(1, ny):
-            with scope("fwait", o, j):
-                f_copy(o, j).wait_recv()
-            total = total + far_in[o - 1, j].astype(F32)
-        out[...] = total * (1.0 / m)
-    for step in range(n - 1):
-        for piece in range(PIECES):
-            for way in range(2):
-                r_copy(step, way, piece).wait_send()
-    for o in range(ny):
-        for j in range(3):
-            n_copy(o, j).wait_send()
-            if o:
-                f_copy(o, j).wait_send()
+    with scope("tail"):
+        sent(n - 3)
+        sent(n - 2)
 
 
 def whole_kernel(n, m, heads, rate, h_in, c_in, wq, wk, wv, dh, dq, dk, dv, *scratch):
@@ -614,9 +674,7 @@
     )
     with scope("chain"):
         chain_phase(heads, rate, c_all, p_all, g_all, *decays[2:], acc, s_term, r_term, state, back)
-    scatter_phase(n, m, h_all, w_all, g_all, dh, dq, dk, dv, *rest)
-    with scope("drain"):
-        drain()
+    scatter_phase(n, m, drain, h_all, w_all, g_all, dh, dq, dk, dv, *rest)
 
 
 def whole(n, m, rate, h, c, wq, wk, wv):
@@ -671,7 +729,7 @@
             pltpu.VMEM((ny, 3, depth, columns), BF16),
             pltpu.VMEM((ny - 1, 3, depth, columns), BF16),
             pltpu.VMEM((ny - 1, 3, depth, columns), BF16),
-            dma((n - 1, 2, PIECES)),
+            dma((n - 1,)),
             dma((n - 1, 2, PIECES)),
             dma((ny, 3)),
             dma((ny, 3)),

time: 112 us -> 107 us (0.955)
  Pallas kernels: 111 us -> 106 us
    pallas_call x1, Pallas kernels: 109 us -> 104 us  [whole(): pl.pallas_call(functools.partial(whole_kernel, n, m, heads), out_shape=(p...]
where the time goes in v3:
time: 107 us
  Pallas kernels  106 us (99%)
    pallas_call x1, Pallas kernels, whole(): pl.pallas_call(functools.partial(whole_kernel, n, m, heads), out_shape=(p...  104 us

profile of v3, /device:TPU:0, one launch (start us, length us, event | category | flops | bytes accessed | tf_op | source)
XLA Modules:
  0.0 107.0 jit_solution(1005664036703581120)
XLA Ops:
  0.6 104.3 %whole.1 = (bf16[128,2048]{1,0:T(8,128)(2,1)S(1)}, f32[512,512]{1,0:T(8,128)S(1)}, f32[512,512]{1,0:T(8,128)S(1)}, f32[512,512]{1,0:T(8,128)S(1)}) custom-call(f32[2]{0:T(128)} %rate.1, bf16[128,2048]{1,0:T(8,128)(2,1)} %bitcast.4, bf16[128,4096]{1,0:T(8,128)(2,1)} %bitcast.3, bf16[512,512]{1,0:T(8,128)(2,1)} %wq.1, bf16[512,512]{1,0:T(8,128)(2,1)} %wk.1, ...), custom_call_target="tpu_custom_call" | custom-call | tf_op jit(solution)/shard_map/whole/pallas_call | solution.py:689
  104.9 1.9 %finish.1 = (bf16[128,2048]{1,0:T(8,128)(2,1)}, f32[512,512]{1,0:T(8,128)}, f32[512,512]{1,0:T(8,128)}, f32[512,512]{1,0:T(8,128)}) custom-call(bf16[128,2048]{1,0:T(8,128)(2,1)S(1)} %get-tuple-element.12.refs_0_, f32[512,512]{1,0:T(8,128)S(1)} %get-tuple-element.13.refs_1_, f32[512,512]{1,0:T(8,128)S(1)} %get-tuple-element.14.refs_2_, ...), custom_call_target="tpu_custom_call" | custom-call | tf_op jit(solution)/shard_map/finish/pallas_call | solution.py:757

commit v4 on v3

--- a/solution.py
+++ b/solution.py
@@ -49,8 +49,9 @@
 
 
 def gather_phase(
-    n, m, project, local, tables, h_in, c_in, wq, wk, wv, h_all, c_all, w_all, c_own, c_via, l_sem,
-    h_recv, h_line, h_side, h_bridge, c_send, c_recv, v_send, v_recv, w_far, w_near, w_recv,
+    n, m, project, local, tables, rate_in, rate, h_in, c_in, wq, wk, wv, h_all, c_all, w_all,
+    c_own, c_via, l_sem,
+    h_recv, h_sent, c_sent, c_recv, v_sent, v_recv, w_sent, w_near, w_recv,
 ):
     s = lax.axis_index("sp")
     d = lax.axis_index("dp")
@@ -70,26 +71,27 @@
     def far(o):
         return ((y + o) % ny) * 2 + core
 
+    def part_rows(block):
+        return pl.ds(pl.multiple_of(block * rows, rows), rows)
+
+    def part_columns(block):
+        return pl.ds(pl.multiple_of(block * columns, columns), columns)
+
+    own_depth = pl.ds(pl.multiple_of(d * depth, depth), depth)
+    loads = [pltpu.make_async_copy(h_in, h_all.at[part_rows(s)], l_sem.at[0])]
+    loads[0].start()
     arrived = greet(
         [{"sp": side}, {"dp": mate}] + [{"dp": far(o)} for o in range(1, ny)],
         [(z >= 1, {"sp": s - 2}), (z + 1 < nz, {"sp": s + 2})],
     )
-
-    def part_rows(block):
-        return pl.ds(pl.multiple_of(block * rows, rows), rows)
-
-    def part_columns(block):
-        return pl.ds(pl.multiple_of(block * columns, columns), columns)
-
-    own_depth = pl.ds(pl.multiple_of(d * depth, depth), depth)
-    loads = [pltpu.make_async_copy(h_in, h_all.at[part_rows(s)], l_sem.at[0])]
     for j, w in enumerate((wq, wk, wv)):
         place = w_all.at[own_depth, pl.ds(j * columns, columns)]
         loads.append(pltpu.make_async_copy(w, place, l_sem.at[1 + j]))
     loads.append(pltpu.make_async_copy(c_in, c_own, l_sem.at[4]))
     mine = c_in.at[:, part_columns(s)]
     loads.append(pltpu.make_async_copy(mine, c_all.at[part_rows(s)], l_sem.at[5]))
-    for load in loads:
+    loads.append(pltpu.make_async_copy(rate_in, rate, l_sem.at[6]))
+    for load in loads[1:]:
         load.start()
 
     def h_copy(src_z, src_x, sub, dest, send):
@@ -97,20 +99,29 @@
         place = pl.ds(pl.multiple_of(block * rows + sub * sub_rows, sub_rows), sub_rows)
         return remote(h_all.at[place], h_all.at[place], send, h_recv.at[block, sub], {"sp": dest})
 
-    def w_copy(src_d, j, dest, send):
+    def w_copy(src_d, j, dest, send, recv):
         place = w_all.at[
             pl.ds(pl.multiple_of(src_d * depth, depth), depth), pl.ds(j * columns, columns)
         ]
-        return remote(place, place, send, w_recv.at[src_d, j], {"dp": dest})
+        return remote(place, place, send, recv, {"dp": dest})
+
+    def w_far_copy(src_d, j, dest):
+        return w_copy(src_d, j, dest, w_sent.at[0], w_recv.at[src_d // 2, j])
+
+    def w_near_copy(src_d, j):
+        return w_copy(src_d, j, mate, w_sent.at[1], w_near.at[j])
+
+    def wait_bytes(ref, sem):
+        pltpu.make_async_copy(ref, ref, sem).wait()
 
     def c_copy(to):
         return remote(
-            c_own.at[:, part_columns(to)], c_all.at[part_rows(s)], c_send.at[to], c_recv.at[s], {"sp": to}
+            c_own.at[:, part_columns(to)], c_all.at[part_rows(s)], c_sent, c_recv.at[s], {"sp": to}
         )
 
     def c_arrival(block):
         return remote(
-            c_all.at[part_rows(block)], c_all.at[part_rows(block)], c_send.at[block], c_recv.at[block], {"sp": side}
+            c_all.at[part_rows(block)], c_all.at[part_rows(block)], c_sent, c_recv.at[block], {"sp": side}
         )
 
     def end_block(e, column):
@@ -119,18 +130,18 @@
     def c_cross(e):
         to = end_block(e, 1 - x)
         return remote(
-            c_own.at[:, part_columns(to)], c_via.at[e], c_send.at[to], v_recv.at[e], {"sp": side}
+            c_own.at[:, part_columns(to)], c_via.at[e], c_sent, v_recv.at[e], {"sp": side}
         )
 
     def c_pass(e):
         return remote(
-            c_via.at[e], c_all.at[part_rows(side)], v_send.at[e], c_recv.at[side], {"sp": end_block(e, x)}
+            c_via.at[e], c_all.at[part_rows(side)], v_sent, c_recv.at[side], {"sp": end_block(e, x)}
         )
 
     def line(k, sub, up):
         source = (z - k) if up else (z + k)
         dest = (s + 2) if up else (s - 2)
-        return h_copy(source, x, sub, dest, h_line.at[k, sub, int(up)])
+        return h_copy(source, x, sub, dest, h_sent.at[0])
 
     def goes(k, up):
         if up:
@@ -147,7 +158,7 @@
         return jnp.logical_and(here, (z != 1) if up else (z != nz - 2))
 
     def bridge(sub):
-        return h_copy(z, 1 - x, sub, inward, h_bridge.at[sub])
+        return h_copy(z, 1 - x, sub, inward, h_sent.at[1])
 
     with scope("greet"):
         loads[0].wait()
@@ -159,12 +170,12 @@
             def _():
                 line(0, sub, up).start()
 
-        h_copy(z, x, sub, side, h_side.at[0, sub, 0]).start()
+        h_copy(z, x, sub, side, h_sent.at[1]).start()
     for j in range(3):
         loads[1 + j].wait()
         for o in range(1, ny):
-            w_copy(d, j, far(o), w_far.at[o, j]).start()
-        w_copy(d, j, mate, w_near.at[0, j]).start()
+            w_far_copy(d, j, far(o)).start()
+        w_near_copy(d, j).start()
     loads[4].wait()
     loads[5].wait()
     if bridged:
@@ -175,13 +186,14 @@
                 c_cross(e).start()
             c_copy(side).start()
 
+    loads[6].wait()
     tables()
 
     def pass_weights(j):
         for o in range(1, ny):
             with scope("wfar", j):
-                w_copy(far(o), j, mate, w_near.at[o, j]).wait_recv()
-            w_copy(far(o), j, mate, w_near.at[o, j]).start()
+                w_far_copy(far(o), j, mate).wait_recv()
+            w_near_copy(far(o), j).start()
 
     def send_level(k):
         for up in (True, False):
@@ -227,14 +239,11 @@
             @pl.when(fresh)
             def _():
                 for sub in range(SUBS):
-                    h_copy(zz, 1 - x, sub, side, h_side.at[0, sub, 0]).wait_recv()
+                    h_copy(zz, 1 - x, sub, side, h_sent.at[1]).wait_recv()
 
     def wait_weights(j):
-        w_copy(mate, j, mate, w_near.at[0, j]).wait_recv()
-        for o in range(1, ny):
-            other = far(o) + 1 - 2 * core
-            with scope("wmate", j):
-                w_copy(other, j, mate, w_near.at[o, j]).wait_recv()
+        with scope("wmate", j):
+            wait_bytes(w_all.at[pl.ds(0, ny * depth), pl.ds(j * columns, columns)], w_near.at[j])
 
     def early():
         for j in range(2):
@@ -263,12 +272,12 @@
                 def _():
                     source = (z - k) if up else (z + k)
                     with scope("hline", k, sub, up):
-                        h_copy(source, x, sub, side, h_side.at[k, sub, int(up)]).wait_recv()
+                        h_copy(source, x, sub, side, h_sent.at[1]).wait_recv()
 
                 @pl.when(crosses(k, up))
                 def _():
                     source = (z - k) if up else (z + k)
-                    h_copy(source, x, sub, side, h_side.at[k, sub, int(up)]).start()
+                    h_copy(source, x, sub, side, h_sent.at[1]).start()
 
                 @pl.when(goes(k, up))
                 def _():
@@ -278,7 +287,7 @@
 
                 @pl.when(is_end)
                 def _():
-                    h_copy(z, 1 - x, sub, side, h_side.at[0, sub, 0]).wait_recv()
+                    h_copy(z, 1 - x, sub, side, h_sent.at[1]).wait_recv()
                     bridge(sub).start()
 
             if bridged and (k, sub) in ((nz - 2, 0), (nz - 2, SUBS - 1), (nz - 1, 0)):
@@ -363,39 +372,27 @@
                 local(zz * 2, zz * 2 + 1)
 
     def drain():
-        for k in range(1, n):
-            c_copy((s + k) % n).wait_send()
-        for j in range(3):
-            for o in range(ny):
-                w_copy(d, j, mate, w_near.at[o, j]).wait_send()
-                if o:
-                    w_copy(d, j, far(o), w_far.at[o, j]).wait_send()
+        wait_bytes(c_all.at[pl.ds(0, (n - 1) * rows)], c_sent)
+        wait_bytes(w_all.at[pl.ds(0, (ny - 1) * depth)], w_sent.at[0])
+        wait_bytes(w_all.at[pl.ds(0, ny * depth)], w_sent.at[1])
         if bridged:
 
             @pl.when(inner)
             def _():
-                for e in range(2):
-                    c_pass(e).wait_send()
-
-            @pl.when(is_end)
-            def _():
-                for sub in range(SUBS):
-                    bridge(sub).wait_send()
-
-        for sub in range(SUBS):
-            h_copy(z, x, sub, side, h_side.at[0, sub, 0]).wait_send()
-            for up in (True, False):
-                for k in range(nz):
-
-                    @pl.when(goes(k, up))
-                    def _():
-                        line(k, sub, up).wait_send()
-
-                    if k:
-
-                        @pl.when(crosses(k, up))
-                        def _():
-                            h_copy(z, x, sub, side, h_side.at[k, sub, int(up)]).wait_send()
+                wait_bytes(c_via, v_sent)
+
+        for zz in range(nz):
+            lines = (zz + 1 if zz + 1 < nz else 0) + (nz - zz if zz else 0)
+            sides = nz
+            if bridged and 0 < zz < nz - 1:
+                sides -= (zz == 1) + (zz == nz - 2)
+            elif bridged:
+                sides += 1
+
+            @pl.when(z == zz)
+            def _():
+                wait_bytes(h_all.at[pl.ds(0, lines * rows)], h_sent.at[0])
+                wait_bytes(h_all.at[pl.ds(0, sides * rows)], h_sent.at[1])
 
     return drain
 
@@ -438,7 +435,7 @@
         mixed = (dot(c, v, NT) * inner[h]).astype(BF16)
         mixed_t = (dot(v, c, NT) * inner_t[h]).astype(BF16)
         scores_t = (dot(k, q, NT) * inner_t[h]).astype(BF16)
-        s_term[block, h] = dot((k.astype(F32) * key_decay[h]).astype(BF16), v, TN)
+        s_term[block, h] = dot(v, (k.astype(F32) * key_decay[h]).astype(BF16), TN)
         r_term[block, h] = dot((q.astype(F32) * query_decay[h]).astype(BF16), c, TN)
         acc[at, parts[0]] = dot(mixed, k)
         acc[at, parts[1]] = dot(mixed_t, q)
@@ -450,29 +447,34 @@
     dim = columns // heads
     blocks = length // BLOCK
     scale = dim ** (-0.5)
-    state[...] = jnp.zeros_like(state)
-    back[...] = jnp.zeros_like(back)
-
     for i in range(blocks):
         for h in range(heads):
             block_decay = jnp.exp(jnp.full((1, dim), rate[h] * BLOCK, F32))
             parts = head_parts(columns, dim, h)
 
             at = slice(i * BLOCK, (i + 1) * BLOCK)
-            held = state[h]
-            across = dot(c_all[at, parts[0]], held.astype(BF16), NT) * query_decay[h]
-            g_all[at, parts[0]] = (acc[at, parts[0]] + across).astype(BF16)
-            state[h] = held * block_decay + s_term[i, h]
+            grad_q = acc[at, parts[0]]
+            if i:
+                held = state[h]
+                grad_q = grad_q + dot(c_all[at, parts[0]], held.astype(BF16)) * query_decay[h]
+                state[h] = held * block_decay + s_term[i, h]
+            else:
+                state[h] = s_term[i, h]
+            g_all[at, parts[0]] = grad_q.astype(BF16)
 
             j = blocks - 1 - i
             at = slice(j * BLOCK, (j + 1) * BLOCK)
-            held = back[h]
-            held_bf = held.astype(BF16)
-            across = dot(p_all[at, parts[2]], held_bf, NT) * key_decay[h]
-            g_all[at, parts[1]] = ((acc[at, parts[1]] + across) * scale).astype(BF16)
-            across = dot(p_all[at, parts[1]], held_bf) * key_decay[h]
-            g_all[at, parts[2]] = (acc[at, parts[2]] + across).astype(BF16)
-            back[h] = held * block_decay + r_term[j, h]
+            grad_k, grad_v = acc[at, parts[1]], acc[at, parts[2]]
+            if i:
+                held = back[h]
+                held_bf = held.astype(BF16)
+                grad_k = grad_k + dot(p_all[at, parts[2]], held_bf, NT) * key_decay[h]
+                grad_v = grad_v + dot(p_all[at, parts[1]], held_bf) * key_decay[h]
+                back[h] = held * block_decay + r_term[j, h]
+            else:
+                back[h] = r_term[j, h]
+            g_all[at, parts[1]] = (grad_k * scale).astype(BF16)
+            g_all[at, parts[2]] = grad_v.astype(BF16)
 
 
 def scatter_phase(
@@ -532,7 +534,7 @@
         return remote(
             src,
             ring.at[step, way, piece],
-            r_send.at[step],
+            r_send,
             r_recv.at[step, way, piece],
             {"sp": right if way == 0 else left},
         )
@@ -560,12 +562,12 @@
 
     def n_copy(o, j):
         return remote(
-            near_out.at[o, j], near_in.at[o, j], n_send.at[o, j], n_recv.at[o, j], {"dp": mate}
+            near_out.at[o, j], near_in.at[o, j], n_send, n_recv.at[o, j], {"dp": mate}
         )
 
     def f_copy(o, j):
         return remote(
-            far_out.at[o - 1, j], far_in.at[o - 1, j], f_send.at[o - 1, j], f_recv.at[o - 1, j], {"dp": far(o)}
+            far_out.at[o - 1, j], far_in.at[o - 1, j], f_send, f_recv.at[o - 1, j], {"dp": far(o)}
         )
 
     def near(o, j):
@@ -611,7 +613,6 @@
         for piece in (2 * first, 2 * first + 1):
             r_copy(0, way, piece).start()
     partial(order[0], -2, 2)
-    work()
     partial(order[1], -2, 2)
     work()
     pairs = [(q, pair) for pair in [(-2, 2), (-3, 3), (n // 2, 0)] for q in order]
@@ -623,24 +624,18 @@
                 f_copy(o, j).wait_recv()
             total = total + far_in[o - 1, j].astype(F32)
         out[...] = total * (1.0 / m)
-        for o in range(1, ny):
-            f_copy(o, j).wait_send()
-
-    def sent(step):
-        pltpu.make_async_copy(ring.at[step], ring.at[step], r_send.at[step]).wait()
+
+    def wait_bytes(ref, sem):
+        pltpu.make_async_copy(ref, ref, sem).wait()
 
     def settle():
-        for o in range(ny):
-            for j in range(3):
-                n_copy(o, j).wait_send()
+        wait_bytes(near_out, n_send)
         drain()
 
     for step in range(n - 1):
         for piece in range(PIECES):
             if step == n - 2 and piece != 2:
                 finish_weight(min(piece, 2))
-            if step > 1 and piece == 0:
-                sent(step - 2)
             if step == n - 3 and piece == 0:
                 work(len(tasks))
                 settle()
@@ -655,14 +650,15 @@
             else:
                 work()
     with scope("tail"):
-        sent(n - 3)
-        sent(n - 2)
-
-
-def whole_kernel(n, m, heads, rate, h_in, c_in, wq, wk, wv, dh, dq, dk, dv, *scratch):
+        wait_bytes(far_out, f_send)
+        wait_bytes(ring, r_send)
+
+
+def whole_kernel(n, m, heads, rate_in, h_in, c_in, wq, wk, wv, dh, dq, dk, dv, *scratch):
+    rate, *scratch = scratch
     h_all, c_all, w_all, p_all, g_all, state, back = scratch[:7]
     decays, (acc, s_term, r_term) = scratch[7:11], scratch[11:14]
-    gather_refs, rest = scratch[14:28], scratch[28:]
+    gather_refs, rest = scratch[14:26], scratch[26:]
     columns = wq.shape[1]
     project = functools.partial(
         project_block, h_all, w_all, p_all, h_in.shape[0], columns, (columns // heads) ** (-0.5)
@@ -670,7 +666,8 @@
     local = functools.partial(local_block, heads, c_all, p_all, *decays, acc, s_term, r_term)
     tables = functools.partial(fill_tables, heads, rate, *decays)
     drain = gather_phase(
-        n, m, project, local, tables, h_in, c_in, wq, wk, wv, h_all, c_all, w_all, *gather_refs
+        n, m, project, local, tables, rate_in, rate, h_in, c_in, wq, wk, wv, h_all, c_all, w_all,
+        *gather_refs,
     )
     with scope("chain"):
         chain_phase(heads, rate, c_all, p_all, g_all, *decays[2:], acc, s_term, r_term, state, back)
@@ -690,10 +687,10 @@
         functools.partial(whole_kernel, n, m, heads),
         out_shape=(pltpu.VMEM((rows, width), BF16),)
         + (pltpu.VMEM((depth, columns), F32),) * 3,
-        in_specs=[pl.BlockSpec(memory_space=pltpu.SMEM)]
-        + [pl.BlockSpec(memory_space=pl.ANY)] * 5,
+        in_specs=[pl.BlockSpec(memory_space=pl.ANY)] * 6,
         out_specs=(vmem,) * 4,
         scratch_shapes=[
+            pltpu.SMEM((heads,), F32),
             pltpu.VMEM((length, width), BF16),
             pltpu.VMEM((length, columns), BF16),
             pltpu.VMEM((depth * m, 3 * columns), BF16),
@@ -710,18 +707,16 @@
             pltpu.VMEM((length // BLOCK, heads, dim, dim), F32),
             pltpu.VMEM((rows, columns * n), BF16),
             pltpu.VMEM((2, rows, columns), BF16),
-            dma((6,)),
+            dma((7,)),
             dma((n, SUBS)),
-            dma((n // 2, SUBS, 2)),
-            dma((n // 2, SUBS, 2)),
-            dma((SUBS,)),
+            dma((2,)),
+            dma(()),
             dma((n,)),
-            dma((n,)),
+            dma(()),
             dma((2,)),
             dma((2,)),
+            dma((3,)),
             dma((ny, 3)),
-            dma((ny, 3)),
-            dma((m, 3)),
             pltpu.VMEM((CHUNKS, length, width // CHUNKS), BF16),
             pltpu.VMEM((n - 1, 2, PIECES, rows // 2, width // CHUNKS), BF16),
             pltpu.VMEM((2, depth, length), BF16),
@@ -729,11 +724,11 @@
             pltpu.VMEM((ny, 3, depth, columns), BF16),
             pltpu.VMEM((ny - 1, 3, depth, columns), BF16),
             pltpu.VMEM((ny - 1, 3, depth, columns), BF16),
-            dma((n - 1,)),
+            dma(()),
             dma((n - 1, 2, PIECES)),
+            dma(()),
             dma((ny, 3)),
-            dma((ny, 3)),
-            dma((ny - 1, 3)),
+            dma(()),
             dma((ny - 1, 3)),
         ],
         compiler_params=pltpu.CompilerParams(

time: 107 us -> 106 us (level)
    pallas_call x1, Pallas kernels: 104 us -> 103 us  [whole(): pl.pallas_call(functools.partial(whole_kernel, n, m, heads), out_shape=(p...]
where the time goes in v4:
time: 106 us; the launch traced here: 105 us
  Pallas kernels  105 us (99%)
    pallas_call x1, Pallas kernels, whole(): pl.pallas_call(functools.partial(whole_kernel, n, m, heads), out_shape=(p...  103 us

profile of v4, /device:TPU:0, one launch (start us, length us, event | category | flops | bytes accessed | tf_op | source)
XLA Modules:
  0.0 105.5 jit_solution(9327626064218246597)
XLA Ops:
  0.6 102.8 %whole.1 = (bf16[128,2048]{1,0:T(8,128)(2,1)S(1)}, f32[512,512]{1,0:T(8,128)S(1)}, f32[512,512]{1,0:T(8,128)S(1)}, f32[512,512]{1,0:T(8,128)S(1)}) custom-call(f32[2]{0:T(128)} %rate_in.1, bf16[128,2048]{1,0:T(8,128)(2,1)} %bitcast.4, bf16[128,4096]{1,0:T(8,128)(2,1)} %bitcast.3, bf16[512,512]{1,0:T(8,128)(2,1)} %wq.1, bf16[512,512]{1,0:T(8,128)(2,1)} %wk.1, ...), custom_call_target="tpu_custom_call" | custom-call | tf_op jit(solution)/shard_map/whole/pallas_call | solution.py:686
  103.4 1.9 %finish.1 = (bf16[128,2048]{1,0:T(8,128)(2,1)}, f32[512,512]{1,0:T(8,128)}, f32[512,512]{1,0:T(8,128)}, f32[512,512]{1,0:T(8,128)}) custom-call(bf16[128,2048]{1,0:T(8,128)(2,1)S(1)} %get-tuple-element.12.refs_0_, f32[512,512]{1,0:T(8,128)S(1)} %get-tuple-element.13.refs_1_, f32[512,512]{1,0:T(8,128)S(1)} %get-tuple-element.14.refs_2_, ...), custom_call_target="tpu_custom_call" | custom-call | tf_op jit(solution)/shard_map/finish/pallas_call | solution.py:752

commit v5 on v4

--- a/solution.py
+++ b/solution.py
@@ -341,12 +341,22 @@
 
     @pl.loop(0, 2 * nz - 1)
     def _(t):
-        last = 2 * nz - 4
-        held = jnp.logical_and(t != last, jnp.logical_or(t == 0, t >= nz - 1))
-        mixes = jnp.where(is_end, held, t % 2 == 0)
-        late = jnp.where(t < nz - 1, t, jnp.where(t < last, t - nz + 2, t - nz + 1))
-        late = jnp.where(t == last, nz - 1, late)
-        zz = level(jnp.where(is_end, late, (t + 1) // 2))
+        inside = jnp.logical_and(t >= nz - 1, t < 2 * nz - 2)
+        middle = jnp.logical_and(jnp.logical_and(is_end, inside), t != max(2 * nz - 4, 1))
+        outer = jnp.logical_or(t == 0, t == 2 * nz - 2)
+        mixes = jnp.where(is_end, jnp.logical_or(outer, middle), t % 2 == 0)
+        at_end = jnp.where(t < nz - 1, t, nz - 1)
+        zz = level(jnp.where(is_end, at_end, (t + 1) // 2))
+
+        def unit(u):
+            column = jnp.where(u < nz - 2, x, 1 - x)
+            return level(1 + u % max(nz - 2, 1)) * 2 + column
+
+        first = 2 * jnp.clip(t - (nz - 1), 0, max(nz - 3, 0))
+        blocks = [
+            jnp.where(middle, unit(first), zz * 2 + x),
+            jnp.where(middle, unit(first + 1), zz * 2 + 1 - x),
+        ]
         if bridged:
 
             @pl.when(jnp.logical_and(is_end, t == 1))
@@ -362,14 +372,14 @@
         @pl.when(mixes)
         def _():
             with scope("cwait"):
-                for column in range(2):
-
-                    @pl.when(zz * 2 + column != s)
+                for block in blocks:
+
+                    @pl.when(block != s)
                     def _():
-                        c_arrival(zz * 2 + column).wait_recv()
+                        c_arrival(block).wait_recv()
 
             with scope("local"):
-                local(zz * 2, zz * 2 + 1)
+                local(*blocks)
 
     def drain():
         wait_bytes(c_all.at[pl.ds(0, (n - 1) * rows)], c_sent)

time: 106 us -> 105 us (level)
  no operation moved by 1% of the time
where the time goes in v5:
time: 105 us
  Pallas kernels  105 us (100%)
    pallas_call x1, Pallas kernels, whole(): pl.pallas_call(functools.partial(whole_kernel, n, m, heads), out_shape=(p...  103 us

profile of v5, /device:TPU:0, one launch (start us, length us, event | category | flops | bytes accessed | tf_op | source)
XLA Modules:
  0.0 105.3 jit_solution(8973691487250590154)
XLA Ops:
  0.6 102.6 %whole.1 = (bf16[128,2048]{1,0:T(8,128)(2,1)S(1)}, f32[512,512]{1,0:T(8,128)S(1)}, f32[512,512]{1,0:T(8,128)S(1)}, f32[512,512]{1,0:T(8,128)S(1)}) custom-call(f32[2]{0:T(128)} %rate_in.1, bf16[128,2048]{1,0:T(8,128)(2,1)} %bitcast.4, bf16[128,4096]{1,0:T(8,128)(2,1)} %bitcast.3, bf16[512,512]{1,0:T(8,128)(2,1)} %wq.1, bf16[512,512]{1,0:T(8,128)(2,1)} %wk.1, ...), custom_call_target="tpu_custom_call" | custom-call | tf_op jit(solution)/shard_map/whole/pallas_call | solution.py:696
  103.3 1.9 %finish.1 = (bf16[128,2048]{1,0:T(8,128)(2,1)}, f32[512,512]{1,0:T(8,128)}, f32[512,512]{1,0:T(8,128)}, f32[512,512]{1,0:T(8,128)}) custom-call(bf16[128,2048]{1,0:T(8,128)(2,1)S(1)} %get-tuple-element.12.refs_0_, f32[512,512]{1,0:T(8,128)S(1)} %get-tuple-element.13.refs_1_, f32[512,512]{1,0:T(8,128)S(1)} %get-tuple-element.14.refs_2_, ...), custom_call_target="tpu_custom_call" | custom-call | tf_op jit(solution)/shard_map/finish/pallas_call | solution.py:762
